TPU v7x, 32 devices: a whole 2x2x4 slice. The times are simulated.
32 devices in a mesh: dp: 4 (over y, x), kv: 4 (over z), tp: 2 (over core).
Axes of the slice: x: 2, y: 2, z: 4, core: 2. Of those that a mesh axis runs over, the one named last changes fastest.
Arguments:
- tokens: bfloat16 [16, 4096], P('dp', ('kv', 'tp')), may hold values from -75 to 75, as said below
- attn_gain: bfloat16 [4096], P('kv'), may hold values from 0.099609375 to 1.8984375
- w_query: bfloat16 [4096, 2048], P('kv', 'tp'), may hold values from -0.09375 to 0.09375
- w_key: bfloat16 [4096, 256], P('kv', 'tp'), may hold values from -0.75 to 0.75
- w_value: bfloat16 [4096, 256], P('kv', 'tp'), may hold values from -0.09375 to 0.09375
- key_cache: bfloat16 [16, 8192, 2, 128], P('dp', 'kv', 'tp'), may hold values from -700 to 700
- value_cache: bfloat16 [16, 8192, 2, 128], P('dp', 'kv', 'tp'), may hold values from -6 to 6
- lam: float32 [16], P('tp'), may hold values from 0.3 to 0.8
- head_gain: bfloat16 [128], replicated, may hold values from 0.099609375 to 1.8984375
- w_out: bfloat16 [2048, 4096], P('tp', 'kv'), may hold values from -0.125 to 0.125
- ffn_gain: bfloat16 [4096], replicated, may hold values from 0.099609375 to 1.8984375
- w_up: bfloat16 [4096, 16384], P(None, ('dp', 'kv', 'tp')), may hold values from -0.09375 to 0.09375
- w_down: bfloat16 [16384, 4096], P(('dp', 'kv', 'tp')), may hold values from -0.09375 to 0.09375
Outputs:
- updated: bfloat16 [16, 4096], P('dp', ('kv', 'tp'))
Inputs may be any that keep to these rules, and one draw needn't show every extreme that they name: `tokens`: column scales differ across the width.
All inputs are finite; a program needn't handle non-finite values.
Results may differ from a plain program's by a relative error of at most 0.017.
Values may be sent and summed in bfloat16 or wider, within the bound.
No kernel may reach another device: no remote copies, remote signals or barrier semaphores. Data moves between devices by JAX's collectives and lax.ppermute only.
A program may use at most 64 MiB of HBM per device.

v0:
```python
import jax
import jax.numpy as jnp
from jax import lax
from jax.sharding import PartitionSpec as P

D = 4096
HD = 64
VD = 128


EPS = 1e-06
THETA = 500000.0
OUT_SCALE = 0.8


def joined(shard, axis, combine):
    everything = jax.tree.map(
        lambda part, kind: lax.all_gather(part.astype(kind), axis),
        shard,
        (jnp.bfloat16, jnp.bfloat16, jnp.bfloat16),
    )

    def take(k):
        return jax.tree.map(lambda part, own: part[k].astype(own.dtype), everything, shard)

    return lax.fori_loop(
        1, lax.axis_size(axis), lambda k, so_far: combine(so_far, take(k)), take(0)
    )


def settle(value):
    return lax.optimization_barrier(value.astype(jnp.bfloat16)).astype(jnp.float32)


def rotate(value, position):
    half = value.shape[-1] // 2
    inverse = THETA ** (-jnp.arange(half, dtype=jnp.float32) * 2.0 / value.shape[-1])
    angle = position * inverse
    cosine = jnp.cos(angle)
    sine = jnp.sin(angle)
    first = value[..., :half]
    second = value[..., half:]
    return jnp.concatenate(
        [first * cosine - second * sine, second * cosine + first * sine], axis=-1
    )


def combine_partials(first, second):
    top_a, den_a, num_a = first
    top_b, den_b, num_b = second
    top = jnp.maximum(top_a, top_b)
    factor_a = jnp.exp(top_a - top)
    factor_b = jnp.exp(top_b - top)
    return (
        top,
        den_a * factor_a + den_b * factor_b,
        num_a * factor_a[..., None] + num_b * factor_b[..., None],
    )


def local(
    tokens,
    attn_gain,
    w_query,
    w_key,
    w_value,
    key_cache,
    value_cache,
    lam,
    head_gain,
    w_out,
    ffn_gain,
    w_up,
    w_down,
):
    f32 = jnp.float32
    bf = jnp.bfloat16
    rows, width = tokens.shape
    kv_count = lax.axis_size("kv")
    tp_count = lax.axis_size("tp")
    dp_count = lax.axis_size("dp")
    positions = key_cache.shape[1]
    kv_local = key_cache.shape[2]
    heads_local = lam.shape[0]
    group = heads_local // kv_local
    scale = HD ** (-0.5)
    slab = lax.all_gather(tokens, "tp", axis=1, tiled=True)
    slab_f = slab.astype(f32)
    scaled = (slab_f * attn_gain.astype(f32)).astype(bf)
    part_q = jnp.dot(scaled, w_query, preferred_element_type=f32)
    part_k = jnp.dot(scaled, w_key, preferred_element_type=f32)
    part_v = jnp.dot(scaled, w_value, preferred_element_type=f32)
    local_sq = jnp.sum(slab_f * slab_f, axis=-1, keepdims=True)
    part_q, part_k, part_v, total_sq = lax.psum((part_q, part_k, part_v, local_sq), "kv")
    inv_rms = lax.rsqrt(total_sq / D + EPS)
    position = jnp.asarray(positions * kv_count, f32)
    query = rotate((part_q * inv_rms).reshape(rows, kv_local, group, 2, HD), position).astype(bf)
    new_key = rotate((part_k * inv_rms).reshape(rows, kv_local, 2, HD), position).astype(bf)
    new_value = (part_v * inv_rms).astype(bf).reshape(rows, kv_local, VD)
    cached_keys = key_cache.reshape(rows, positions, kv_local, 2, HD)
    scores = (
        jnp.einsum("rkgmd,rpkmd->rkgmp", query, cached_keys, preferred_element_type=f32) * scale
    )
    local_top = jnp.max(scores, axis=-1)
    expo = jnp.exp(scores - local_top[..., None])
    local_den = jnp.sum(expo, axis=-1)
    local_num = jnp.einsum(
        "rkgmp,rpkv->rkgmv", expo.astype(bf), value_cache, preferred_element_type=f32
    )
    top, den, num = joined((local_top, local_den, local_num), "kv", combine_partials)
    own_score = jnp.einsum("rkgmd,rkmd->rkgm", query, new_key, preferred_element_type=f32) * scale
    final_top = jnp.maximum(top, own_score)
    carried = jnp.exp(top - final_top)
    own_weight = jnp.exp(own_score - final_top)
    den = den * carried + own_weight
    num = (
        num * carried[..., None]
        + settle(own_weight)[..., None] * new_value.astype(f32)[:, :, None, None, :]
    )
    lam_h = lam.reshape(kv_local, group)
    mix = (
        num[..., 0, :] / den[..., 0, None]
        - lam_h[None, :, :, None] * num[..., 1, :] / den[..., 1, None]
    )
    normed = (
        mix
        * lax.rsqrt(jnp.mean(mix * mix, axis=-1, keepdims=True) + EPS)
        * head_gain.astype(f32)
        * OUT_SCALE
    )
    attended = normed.astype(bf).reshape(rows, heads_local * VD)
    part_out = jnp.dot(attended, w_out, preferred_element_type=f32)
    branch = lax.psum_scatter(
        part_out.astype(jnp.bfloat16), "tp", scatter_dimension=1, tiled=True
    ).astype(jnp.float32)
    hidden = (tokens.astype(f32) + branch).astype(bf)
    everyone = lax.all_gather(hidden[None], ("dp", "kv", "tp"), axis=0, tiled=True)
    blocks = kv_count * tp_count
    grid = everyone.reshape(dp_count, blocks, rows, width).astype(f32)
    row_sq = jnp.sum(grid * grid, axis=(1, 3))
    inv_two = lax.rsqrt(row_sq / D + EPS)
    gains = ffn_gain.astype(f32).reshape(blocks, width)
    normed_two = (grid * inv_two[:, None, :, None] * gains[None, :, None, :]).astype(bf)
    upward = jnp.einsum(
        "acrd,cdf->arf",
        normed_two,
        w_up.reshape(blocks, width, w_up.shape[1]),
        preferred_element_type=f32,
    )
    act = jnp.square(jax.nn.relu(upward)).astype(bf)
    down = jnp.einsum(
        "arf,fcd->acrd",
        act,
        w_down.reshape(w_down.shape[0], blocks, width),
        preferred_element_type=f32,
    )
    term = down.reshape(dp_count * blocks * rows, width)
    mixed = lax.psum_scatter(term, ("dp", "kv", "tp"), scatter_dimension=0, tiled=True)
    return (lax.optimization_barrier(hidden).astype(f32) + mixed).astype(bf)


def solution(mesh):
    in_specs = (
        P("dp", ("kv", "tp")),
        P("kv"),
        P("kv", "tp"),
        P("kv", "tp"),
        P("kv", "tp"),
        P("dp", "kv", "tp", None),
        P("dp", "kv", "tp", None),
        P("tp"),
        P(),
        P("tp", "kv"),
        P(),
        P(None, ("dp", "kv", "tp")),
        P(("dp", "kv", "tp"), None),
    )
    out_specs = P("dp", ("kv", "tp"))
    return jax.shard_map(local, mesh=mesh, in_specs=in_specs, out_specs=out_specs, check_vma=False)
```

profile of v0, /device:TPU:0, one launch (start us, length us, event | category | flops | bytes accessed | tf_op | source)
XLA Modules:
  0.0 269.8 jit_solution(11153000888686022137)
XLA Ops:
  6.6 2.2 all_gather.20
  8.8 0.7 convert_element_type.215
  9.5 0.1 fusion.27
  9.6 2.0 fusion.56
  11.6 0.1 fusion.52
  11.8 0.2 fusion.54
  11.9 20.6 %all-reduce.1 = (f32[4,1024]{1,0:T(4,128)S(1)}, f32[4,1]{0,1:T(1,128)S(1)}, f32[4,128]{1,0:T(4,128)S(1)}, f32[4,128]{1,0:T(4,128)S(1)}) all-reduce(f32[4,1024]{1,0:T(4,128)S(1)} %fusion.56, f32[4,1]{0,1:T(1,128)S(1)} %bitcast.225, f32[4,128]{1,0:T(4,128)S(1)} %fusion.52, ...), channel_id=1, replica_groups=mesh['dp'=4,'kv'=4,'tp'=2] {'kv'}, use_global_device_ids=true, to_apply=%region_0.0 | all-reduce | flops 5124 | bytes 40992 | tf_op jit(solution)/shard_map/psum | solution.py:94
  32.8 4.0 %copy.80 = bf16[4,2048,1,128]{1,3,0,2:T(8,128)(2,1)} copy(bf16[4,2048,1,128]{3,1,2,0:T(8,128)(2,1)} %param.20) | data formatting | bytes 4194304 | tf_op args[5]
  36.8 2.1 fusion.65
  38.9 0.2 fusion.19
  39.2 0.4 fusion.14
  39.6 13.1 %all-gather.2 = bf16[16,8,2,128]{3,1,2,0:T(8,128)(2,1)S(1)} all-gather(bf16[4,8,2,128]{3,1,2,0:T(8,128)(2,1)S(1)} %fusion.14), channel_id=4, replica_groups=mesh['dp'=4,'kv'=4,'tp'=2] {'kv'}, dimensions={0}, use_global_device_ids=true | all-gather | bytes 81920 | tf_op jit(solution)/shard_map/all_gather | solution.py:18
  52.8 11.9 %all-gather.1 = bf16[16,8,2]{1,2,0:T(2,128)(2,1)S(1)} all-gather(bf16[4,8,2]{1,2,0:T(2,128)(2,1)S(1)} %fusion.19), channel_id=3, replica_groups=mesh['dp'=4,'kv'=4,'tp'=2] {'kv'}, dimensions={0}, use_global_device_ids=true | all-gather | bytes 640 | tf_op jit(solution)/shard_map/all_gather | solution.py:18
  64.8 11.9 %all-gather = bf16[16,8,2]{1,2,0:T(2,128)(2,1)S(1)} all-gather(bf16[4,8,2]{1,2,0:T(2,128)(2,1)S(1)} %convert_element_type.217), channel_id=2, replica_groups=mesh['dp'=4,'kv'=4,'tp'=2] {'kv'}, dimensions={0}, use_global_device_ids=true | all-gather | bytes 640 | tf_op jit(solution)/shard_map/all_gather | solution.py:18
  76.7 1.6 while.19
  77.0 0.2 fusion.78
  77.5 0.2 fusion.78
  78.0 0.2 fusion.78
  78.6 0.2 fusion.43
  79.0 0.1 multiply_add_fusion
  79.4 0.2 multiply_reduce_fusion
  79.7 2.0 convolution_convert_fusion
  81.7 0.9 copy.107
  82.7 6.4 %reduce-scatter.4.cloned.1.call-done = bf16[512,4]{1,0:T(8,128)(2,1)} async-done(((bf16[1024,4]{1,0:T(8,128)(2,1)}), bf16[512,4]{1,0:T(8,128)(2,1)}) %reduce-scatter.4.cloned.1.call-update) | async-done | bytes 4112
  89.1 1.0 copy.108
  90.1 42.2 %all-gather.4 = bf16[32,4,512]{2,1,0:T(4,128)(2,1)S(1)} all-gather(bf16[1,4,512]{2,1,0:T(4,128)(2,1)S(1)} %bitcast.223), channel_id=5, replica_groups=mesh['dp'=4,'kv'=4,'tp'=2] {'dp','kv','tp'}, dimensions={0}, use_global_device_ids=true | all-gather | bytes 135168 | tf_op jit(solution)/shard_map/all_gather | solution.py:137
  132.3 0.1 fusion.22
  132.7 0.1 fusion.21
  132.8 4.9 %fusion.10 = f32[4,8,4,512]{3,2,1,0:T(4,128)S(1)} fusion(bf16[64,8,8,512]{3,2,1,0:T(8,128)(2,1)} %bitcast.211, bf16[4,8,4,512]{3,2,1,0:T(4,128)(2,1)S(1)} %bitcast.214, bf16[8,512,512,1]{2,1,0,3:T(8,128)(2,1)} %bitcast.212), kind=kOutput, calls=%fused_computation.23 | convolution fusion | flops 134242304 | bytes 8781824 | tf_op jit(solution)/shard_map/arf,fcd->acrd/dot_general | solution.py:151
  137.7 0.8 reshape.352
  138.5 123.1 %all-reduce.4.cloned.1.call-done = f32[128,512]{1,0:T(8,128)} async-done(((f32[128,512]{1,0:T(8,128)}), f32[128,512]{1,0:T(8,128)}) %all-reduce.4.cloned.1.call-update) | async-done | bytes 262160
  261.7 1.3 fusion.37
  (77 shorter events, 2.4 us)
Async XLA Ops:
  6.5 32.6 %copy-start = (bf16[4,2048,1,128]{3,1,2,0:T(8,128)(2,1)S(1)}, bf16[4,2048,1,128]{3,1,2,0:T(8,128)(2,1)}, u32[]{:S(2)}) copy-start(bf16[4,2048,1,128]{3,1,2,0:T(8,128)(2,1)} %param.21) | copy-start | bytes 6291460
  6.5 5.1 %copy-start.1 = (bf16[1024,128]{1,0:T(8,128)(2,1)S(1)}, bf16[1024,128]{1,0:T(8,128)(2,1)}, u32[]{:S(2)}) copy-start(bf16[1024,128]{1,0:T(8,128)(2,1)} %param.19) | copy-start | bytes 786436
  6.5 5.2 %copy-start.2 = (bf16[1024,128]{1,0:T(8,128)(2,1)S(1)}, bf16[1024,128]{1,0:T(8,128)(2,1)}, u32[]{:S(2)}) copy-start(bf16[1024,128]{1,0:T(8,128)(2,1)} %param.18) | copy-start | bytes 786436
  6.5 82.6 %reduce-scatter.4.cloned.1.call-start = ((), (), s32[]{:S(2)}) async-start(), calls=%async_computation.1 | async-start | bytes 393216
  39.2 40.2 %copy-start.5 = (f32[8]{0:T(128)S(1)}, f32[8]{0:T(128)}, u32[]{:S(2)}) copy-start(f32[8]{0:T(128)} %param.22) | copy-start | bytes 100
  39.2 40.5 %copy-start.6 = (bf16[128]{0:T(256)(128)(2,1)S(1)}, bf16[128]{0:T(256)(128)(2,1)}, u32[]{:S(2)}) copy-start(bf16[128]{0:T(256)(128)(2,1)} %param.23) | copy-start | bytes 772
  76.7 6.0 %copy-start.4 = (bf16[4096]{0:T(1024)(128)(2,1)S(1)}, bf16[4096]{0:T(1024)(128)(2,1)}, u32[]{:S(2)}) copy-start(bf16[4096]{0:T(1024)(128)(2,1)} %param.25) | copy-start | bytes 24580
  78.3 11.8 %copy-start.3 = (bf16[4,512]{1,0:T(4,128)(2,1)S(1)}, bf16[4,512]{1,0:T(4,128)(2,1)}, u32[]{:S(2)}) copy-start(bf16[4,512]{1,0:T(4,128)(2,1)} %param.15) | copy-start | bytes 12292
  82.6 179.0 %all-reduce.4.cloned.1.call-start = ((), (), s32[]{:S(2)}) async-start(), calls=%async_computation.2 | async-start | bytes 524288
Sparse Core Ops, SparseCore 0:
  82.7 6.3 reduce-scatter.3
  138.7 122.9 all-reduce.3
where the time goes:
time: 270 us
  waiting for transfers between devices  130 us (48%)
  blocking collectives  102 us (38%)
  between operations  13.6 us (5%)
  matrix products  11.9 us (4%)
  local copies, waits for them, and re-layouts  8.44 us (3%)
  other arithmetic  4.21 us (2%)
    unnamed x4, waiting for transfers between devices  130 us
    all_gather x1, blocking collectives, local(): lax.all_gather(hidden[None], ('dp', 'kv', 'tp'), axis=0, tiled=True)  42.2 us
    all_gather x3, blocking collectives, joined(): lax.all_gather(part.astype(kind), axis)  37 us
    psum x1, blocking collectives, local(): lax.psum((part_q, part_k, part_v, local_sq), 'kv')  20.6 us
    unnamed x22, local copies, waits for them, and re-layouts  6.33 us
  transfers between devices with their start and end apart: 2, of which 2 were waited for; matrix products, arithmetic and copies ran while one was open for 0% of the time, Pallas kernels for 0%

commit v1 on v0

v1 whole, which is shorter than its diff:
```python
import jax
import jax.numpy as jnp
from jax import lax
from jax.sharding import PartitionSpec as P

D = 4096
HD = 64
VD = 128


EPS = 1e-06
THETA = 500000.0
OUT_SCALE = 0.8


def everyones(value, axis):
    count = lax.axis_size(axis)
    if count > 8:
        copies = jnp.broadcast_to(value[None], (count,) + value.shape)
        got = lax.all_to_all(copies, axis, 0, 0, tiled=True)
        return [got[k] for k in range(count)]
    return [value] + [
        lax.ppermute(value, axis, [(i, (i + step) % count) for i in range(count)])
        for step in range(1, count)
    ]


def split3(value):
    bf = jnp.bfloat16
    f32 = jnp.float32
    high = lax.reduce_precision(value, 8, 7)
    rest = value - high
    middle = lax.reduce_precision(rest, 8, 7)
    low = lax.reduce_precision(rest - middle, 8, 7)
    return [part.astype(bf) for part in (high, middle, low)]


def join3(parts):
    f32 = jnp.float32
    high, middle, low = (part.astype(f32) for part in parts)
    return high + (middle + low)


def settle(value):
    return lax.reduce_precision(value, 8, 7)


def rotate(value, position):
    half = value.shape[-1] // 2
    inverse = THETA ** (-jnp.arange(half, dtype=jnp.float32) * 2.0 / value.shape[-1])
    angle = position * inverse
    cosine = jnp.cos(angle)
    sine = jnp.sin(angle)
    first = value[..., :half]
    second = value[..., half:]
    return jnp.concatenate(
        [first * cosine - second * sine, second * cosine + first * sine], axis=-1
    )


def local(
    tokens,
    attn_gain,
    w_query,
    w_key,
    w_value,
    key_cache,
    value_cache,
    lam,
    head_gain,
    w_out,
    ffn_gain,
    w_up,
    w_down,
):
    f32 = jnp.float32
    bf = jnp.bfloat16
    rows, width = tokens.shape
    kv_count = lax.axis_size("kv")
    tp_count = lax.axis_size("tp")
    dp_count = lax.axis_size("dp")
    me_tp = lax.axis_index("tp")
    positions = key_cache.shape[1]
    kv_local = key_cache.shape[2]
    heads_local = lam.shape[0]
    group = heads_local // kv_local
    scale = HD ** (-0.5)
    axes = ("dp", "kv", "tp")
    assert tp_count == 2
    swap = [(0, 1), (1, 0)]

    other = lax.ppermute(tokens, "tp", swap)
    slab = jnp.where(
        me_tp == 0,
        jnp.concatenate([tokens, other], axis=1),
        jnp.concatenate([other, tokens], axis=1),
    )
    slab_f = slab.astype(f32)
    scaled = (slab_f * attn_gain.astype(f32)).astype(bf)
    part_q = jnp.dot(scaled, w_query, preferred_element_type=f32)
    part_k = jnp.dot(scaled, w_key, preferred_element_type=f32)
    part_v = jnp.dot(scaled, w_value, preferred_element_type=f32)
    local_sq = jnp.sum(slab_f * slab_f, axis=-1, keepdims=True)
    packed = jnp.concatenate(
        [part_q, part_k, part_v, jnp.broadcast_to(local_sq, (rows, 128))], axis=1
    )
    total = sum(everyones(packed, "kv"))
    width_q = part_q.shape[1]
    width_k = part_k.shape[1]
    width_v = part_v.shape[1]
    total_q = total[:, :width_q]
    total_k = total[:, width_q : width_q + width_k]
    total_v = total[:, width_q + width_k : width_q + width_k + width_v]
    total_sq = total[:, width_q + width_k + width_v :][:, :1]
    inv_rms = lax.rsqrt(total_sq / D + EPS)
    position = jnp.asarray(positions * kv_count, f32)
    query = rotate((total_q * inv_rms).reshape(rows, kv_local, group, 2, HD), position).astype(bf)
    new_key = rotate((total_k * inv_rms).reshape(rows, kv_local, 2, HD), position).astype(bf)
    new_value = (total_v * inv_rms).astype(bf).reshape(rows, kv_local, VD)

    zero = jnp.zeros_like(query[..., 0, :])
    wide = jnp.stack(
        [
            jnp.concatenate([query[..., 0, :], zero], axis=-1),
            jnp.concatenate([zero, query[..., 1, :]], axis=-1),
        ],
        axis=3,
    )
    scores = (
        jnp.einsum("rkgmd,rpkd->rkgmp", wide, key_cache, preferred_element_type=f32) * scale
    )
    local_top = jnp.max(scores, axis=-1)
    expo = jnp.exp(scores - local_top[..., None])
    local_den = jnp.sum(expo, axis=-1)
    local_num = jnp.einsum(
        "rkgmp,rpkv->rkgmv", expo.astype(bf), value_cache, preferred_element_type=f32
    )
    parts = split3(local_top) + split3(local_den)
    stats = jnp.stack(parts, axis=0).reshape(len(parts), -1)
    flat_num = local_num.astype(bf).reshape(-1, VD)
    stats = stats.reshape(-1, VD)
    pad = -stats.shape[0] % 16
    message = jnp.concatenate([flat_num, jnp.pad(stats, ((0, pad), (0, 0)))], axis=0)
    tops = []
    dens = []
    nums = []
    for got in everyones(message, "kv"):
        nums.append(got[: flat_num.shape[0]].astype(f32).reshape(local_num.shape))
        held = got[flat_num.shape[0] :][: stats.shape[0]].reshape((len(parts),) + local_top.shape)
        tops.append(join3(held[:3]))
        dens.append(join3(held[3:]))
    own_score = jnp.einsum("rkgmd,rkmd->rkgm", query, new_key, preferred_element_type=f32) * scale
    final_top = own_score
    for top in tops:
        final_top = jnp.maximum(final_top, top)
    own_weight = jnp.exp(own_score - final_top)
    den = own_weight
    num = settle(own_weight)[..., None] * new_value.astype(f32)[:, :, None, None, :]
    for top, den_k, num_k in zip(tops, dens, nums):
        carried = jnp.exp(top - final_top)
        den = den + den_k * carried
        num = num + num_k * carried[..., None]
    lam_h = lam.reshape(kv_local, group)
    mix = (
        num[..., 0, :] / den[..., 0, None]
        - lam_h[None, :, :, None] * num[..., 1, :] / den[..., 1, None]
    )
    normed = (
        mix
        * lax.rsqrt(jnp.mean(mix * mix, axis=-1, keepdims=True) + EPS)
        * head_gain.astype(f32)
        * OUT_SCALE
    )
    attended = normed.astype(bf).reshape(rows, heads_local * VD)
    part_out = jnp.dot(attended, w_out, preferred_element_type=f32).astype(bf)
    low = part_out[:, :width]
    high = part_out[:, width:]
    mine = jnp.where(me_tp == 0, low, high)
    theirs = jnp.where(me_tp == 0, high, low)
    received = lax.ppermute(theirs, "tp", swap)
    branch = mine.astype(f32) + received.astype(f32)
    hidden = (tokens.astype(f32) + branch).astype(bf)
    devices = dp_count * kv_count * tp_count
    everyone = lax.all_to_all(
        jnp.broadcast_to(hidden[None], (devices,) + hidden.shape), axes, 0, 0, tiled=True
    )
    blocks = kv_count * tp_count
    grid = everyone.reshape(dp_count, blocks, rows, width).astype(f32)
    row_sq = jnp.sum(grid * grid, axis=(1, 3))
    inv_two = lax.rsqrt(row_sq / D + EPS)
    gains = ffn_gain.astype(f32).reshape(blocks, width)
    normed_two = (grid * inv_two[:, None, :, None] * gains[None, :, None, :]).astype(bf)
    upward = jnp.einsum(
        "acrd,cdf->arf",
        normed_two,
        w_up.reshape(blocks, width, w_up.shape[1]),
        preferred_element_type=f32,
    )
    act = jnp.square(jax.nn.relu(upward)).astype(bf)
    down = jnp.einsum(
        "arf,fcd->acrd",
        act,
        w_down.reshape(w_down.shape[0], blocks, width),
        preferred_element_type=f32,
    )
    term = down.astype(bf).reshape(devices, rows, width)
    terms = lax.all_to_all(term, axes, 0, 0, tiled=True)
    mixed = jnp.sum(terms.astype(f32), axis=0)
    return (hidden.astype(f32) + mixed).astype(bf)


def solution(mesh):
    in_specs = (
        P("dp", ("kv", "tp")),
        P("kv"),
        P("kv", "tp"),
        P("kv", "tp"),
        P("kv", "tp"),
        P("dp", "kv", "tp", None),
        P("dp", "kv", "tp", None),
        P("tp"),
        P(),
        P("tp", "kv"),
        P(),
        P(None, ("dp", "kv", "tp")),
        P(("dp", "kv", "tp"), None),
    )
    out_specs = P("dp", ("kv", "tp"))
    return jax.shard_map(local, mesh=mesh, in_specs=in_specs, out_specs=out_specs, check_vma=False)
```

time: 270 us -> 59.5 us (0.22)
  waiting for transfers between devices: 130 us -> 14.3 us
  blocking collectives: 102 us -> 9.86 us
  starting transfers between devices: 0.04 us -> 15.5 us
  between operations: 13.6 us -> 0.32 us
  local copies, waits for them, and re-layouts: 8.44 us -> 4.08 us
    unnamed x4 -> x0, waiting for transfers between devices: 130 us -> none
    all_gather x5 -> x0, blocking collectives: 81.4 us -> none  [the longest x1 42.2 us: local(): lax.all_gather(hidden[None], ('dp', 'kv', 'tp'), axis=0, tiled=True)]
    psum x1 -> x0, blocking collectives: 20.6 us -> none  [local(): lax.psum((part_q, part_k, part_v, local_sq), 'kv')]
    ppermute x0 -> x8, starting transfers between devices: none -> 11.2 us  [the longest x6 10.6 us: everyones(): lax.ppermute(value, axis, [(i, (i + step) % count) for i in range(count)])]
    all_to_all x0 -> x1, blocking collectives: none -> 9.86 us  [local(): terms = lax.all_to_all(term, axes, 0, 0, tiled=True)]
    all_to_all x0 -> x1, waiting for transfers between devices: none -> 8.11 us  [local(): lax.all_to_all(jnp.broadcast_to(hidden[None], (devices,) + hidden.shape),...]
    ppermute x0 -> x8, waiting for transfers between devices: none -> 6.18 us  [the longest x6 5.02 us: everyones(): lax.ppermute(value, axis, [(i, (i + step) % count) for i in range(count)])]
    unnamed x22 -> x20, local copies, waits for them, and re-layouts: 6.33 us -> 0.74 us
  transfers between devices with their start and end apart: 2 -> 9, of which waited for: 2 -> 6; matrix products, arithmetic and copies ran while one was open for 0% -> 5% of each run, Pallas kernels for 0% -> 0%
where the time goes in v1:
time: 59.5 us; the launch traced here: 59.1 us
  starting transfers between devices  15.5 us (26%)
  waiting for transfers between devices  14.3 us (24%)
  matrix products  10.5 us (18%)
  blocking collectives  9.86 us (17%)
  other arithmetic  4.54 us (8%)
  local copies, waits for them, and re-layouts  4.08 us (7%)
    ppermute x6, starting transfers between devices, everyones(): lax.ppermute(value, axis, [(i, (i + step) % count) for i in range(count)])  10.6 us
    all_to_all x1, blocking collectives, local(): terms = lax.all_to_all(term, axes, 0, 0, tiled=True)  9.86 us
    all_to_all x1, waiting for transfers between devices, local(): lax.all_to_all(jnp.broadcast_to(hidden[None], (devices,) + hidden.shape),...  8.11 us
    ppermute x6, waiting for transfers between devices, everyones(): lax.ppermute(value, axis, [(i, (i + step) % count) for i in range(count)])  5.02 us
    dot_general x1, matrix products, local(): jnp.einsum('arf,fcd->acrd', act, w_down.reshape(w_down.shape[0], blocks,...  4.88 us
    all_to_all x1, starting transfers between devices, local(): lax.all_to_all(jnp.broadcast_to(hidden[None], (devices,) + hidden.shape),...  4.26 us
    dot_general x1, matrix products, local(): part_q = jnp.dot(scaled, w_query, preferred_element_type=f32)  2.01 us
    dot_general x1, matrix products, local(): part_out = jnp.dot(attended, w_out, preferred_element_type=f32).astype(bf)  1.98 us
  transfers between devices with their start and end apart: 9, of which 6 were waited for; matrix products, arithmetic and copies ran while one was open for 5% of the time, Pallas kernels for 0%

profile of v1, /device:TPU:0, one launch (start us, length us, event | category | flops | bytes accessed | tf_op | source)
XLA Modules:
  0.0 59.1 jit_solution(7400151228716323851)
XLA Ops:
  0.0 0.6 collective-permute-start
  0.6 0.7 %convert_element_type.556 = f32[128]{0:T(128)S(1)} convert(bf16[128]{0:T(256)(128)(2,1)} %param.21) | non-fusion elementwise | flops 128 | bytes 768 | tf_op jit(solution)/shard_map/convert_element_type | solution.py:171
  1.2 0.7 %broadcast_bitcast_fusion.5 = (f32[1024]{0:T(1024)S(1)}, f32[1024]{0:T(1024)S(1)}) fusion(f32[128]{0:T(128)S(1)} %convert_element_type.556, f32[8]{0:T(128)} %param.20), kind=kLoop, calls=%fused_computation.163 | loop fusion | bytes 8736 | tf_op jit(solution)/shard_map/mul | solution.py:169
  2.0 0.7 %convert_element_type.513 = f32[1024]{0:T(1024)S(1)} convert(bf16[1024]{0:T(1024)(128)(2,1)} %param.14) | non-fusion elementwise | flops 1024 | bytes 6144 | tf_op jit(solution)/shard_map/convert_element_type | solution.py:99
  2.6 0.9 %fusion.27 = f32[4]{0:T(128)S(1)} fusion(bf16[4,512]{1,0:T(4,128)(2,1)} %param.13, bf16[4,512]{1,0:T(4,128)(2,1)S(1)} %collective-permute-done, pred[]{:T(512)S(6)} %eq.2), kind=kLoop, calls=%fused_computation.43 | loop fusion | flops 49148 | bytes 8209 | tf_op jit(solution)/shard_map/reduce_sum | solution.py:103
  3.5 2.0 %fusion.80 = f32[4,1024]{1,0:T(4,128)S(1)} fusion(bf16[1024,1024]{1,0:T(8,128)(2,1)} %param.15, f32[1024]{0:T(1024)S(1)} %convert_element_type.513, bf16[4,512]{1,0:T(4,128)(2,1)S(1)} %collective-permute-done, bf16[4,512]{1,0:T(4,128)(2,1)} %param.13, pred[]{:T(512)S(6)} %eq.2), kind=kOutput, calls=%fused_computation.177 | convolution fusion | flops 8437760 | bytes 2125825 | tf_op jit(solution)/shard_map/dot_general | solution.py:100
  5.9 2.8 %collective-permute-start.1 = (f32[4,1408]{1,0:T(4,128)S(1)}, f32[4,1408]{1,0:T(4,128)S(1)}, u32[]{:S(2)}, u32[]{:S(2)}) collective-permute-start(f32[4,1408]{1,0:T(4,128)S(1)} %pad_maximum_fusion), channel_id=1, source_target_pairs={{0,2},{2,4},{4,6},{6,0},{1,3},{3,5},{5,7},{7,1},{8,10},{10,12},{12... | collective-permute-start | bytes 67592 | tf_op jit(solution)/shard_map/ppermute | solution.py:23
  8.7 2.6 %collective-permute-start.2 = (f32[4,1408]{1,0:T(4,128)S(1)}, f32[4,1408]{1,0:T(4,128)S(1)}, u32[]{:S(2)}, u32[]{:S(2)}) collective-permute-start(f32[4,1408]{1,0:T(4,128)S(1)} %pad_maximum_fusion), channel_id=1, source_target_pairs={{0,4},{2,6},{4,0},{6,2},{1,5},{3,7},{5,1},{7,3},{8,12},{10,14},{12... | collective-permute-start | bytes 67592 | tf_op jit(solution)/shard_map/ppermute | solution.py:23
  11.3 1.3 %collective-permute-start.3 = (f32[4,1408]{1,0:T(4,128)S(1)}, f32[4,1408]{1,0:T(4,128)S(1)}, u32[]{:S(2)}, u32[]{:S(2)}) collective-permute-start(f32[4,1408]{1,0:T(4,128)S(1)} %pad_maximum_fusion), channel_id=1, source_target_pairs={{0,6},{2,0},{4,2},{6,4},{1,7},{3,1},{5,3},{7,5},{8,14},{10,8},{12,... | collective-permute-start | bytes 67592 | tf_op jit(solution)/shard_map/ppermute | solution.py:23
  12.7 0.7 %collective-permute-done.2 = f32[4,1408]{1,0:T(4,128)S(1)} collective-permute-done((f32[4,1408]{1,0:T(4,128)S(1)}, f32[4,1408]{1,0:T(4,128)S(1)}, u32[]{:S(2)}, u32[]{:S(2)}) %collective-permute-start.2) | collective-permute-done | bytes 22560 | tf_op jit(solution)/shard_map/ppermute | solution.py:23
  13.4 1.7 %collective-permute-done.3 = f32[4,1408]{1,0:T(4,128)S(1)} collective-permute-done((f32[4,1408]{1,0:T(4,128)S(1)}, f32[4,1408]{1,0:T(4,128)S(1)}, u32[]{:S(2)}, u32[]{:S(2)}) %collective-permute-start.3) | collective-permute-done | bytes 22560 | tf_op jit(solution)/shard_map/ppermute | solution.py:23
  15.8 0.7 %fusion.87 = (f32[4,8,2]{1,2,0:T(2,128)S(1)}, f32[4,8,2,2048]{3,1,2,0:T(8,128)S(1)}) fusion(bf16[4,2048,1,128]{3,1,2,0:T(8,128)(2,1)S(1)} %copy-done, bf16[4,1,8,1,128]{4,2,3,0,1:T(8,128)(2,1)S(1)} %pad_bitcast_fusion, bf16[4,1,8,1,128]{4,2,3,0,1:T(8,128)(2,1)S(1)} %pad_bitcast_fusion.1), kind=kOutput, calls=%fused_computation.183 | convolution fusion | flops 33824704 | bytes 2638080 | tf_op jit(solution)/shard_map/rkgmd,rpkd->rkgmp/dot_general | solution.py:130
  16.5 0.2 fusion.13
  16.8 0.3 copy-done.1
  17.1 0.4 fusion.9
  17.6 0.2 copy.182
  18.0 0.2 collective-permute-start.4
  18.2 3.6 %collective-permute-start.5 = (bf16[80,128]{1,0:T(8,128)(2,1)S(1)}, bf16[80,128]{1,0:T(8,128)(2,1)S(1)}, u32[]{:S(2)}, u32[]{:S(2)}) collective-permute-start(bf16[80,128]{1,0:T(8,128)(2,1)S(1)} %fusion.25), channel_id=1, source_target_pairs={{0,4},{2,6},{4,0},{6,2},{1,5},{3,7},{5,1},{7,3},{8,12},{10,14},{12... | collective-permute-start | bytes 61448 | tf_op jit(solution)/shard_map/ppermute | solution.py:23
  22.2 0.2 fusion.38
  22.4 1.4 %collective-permute-done.4 = bf16[80,128]{1,0:T(8,128)(2,1)S(1)} collective-permute-done((bf16[80,128]{1,0:T(8,128)(2,1)S(1)}, bf16[80,128]{1,0:T(8,128)(2,1)S(1)}, u32[]{:S(2)}, u32[]{:S(2)}) %collective-permute-start.4) | collective-permute-done | bytes 20512 | tf_op jit(solution)/shard_map/ppermute | solution.py:23
  24.0 0.2 reshape.804
  24.4 1.2 %collective-permute-done.6 = bf16[80,128]{1,0:T(8,128)(2,1)S(1)} collective-permute-done((bf16[80,128]{1,0:T(8,128)(2,1)S(1)}, bf16[80,128]{1,0:T(8,128)(2,1)S(1)}, u32[]{:S(2)}, u32[]{:S(2)}) %collective-permute-start.6) | collective-permute-done | bytes 20512 | tf_op jit(solution)/shard_map/ppermute | solution.py:23
  25.6 0.2 reshape.805
  26.5 0.2 fusion.40
  26.8 2.0 %convolution_convert_fusion = bf16[4,1024]{1,0:T(4,128)(2,1)S(1)} fusion(bf16[1024,1024]{1,0:T(8,128)(2,1)} %param.22, f32[1,4,8,128]{3,2,1,0:T(8,128)S(1)} %broadcast_bitcast_fusion.2, f32[1,4,8,128]{3,2,1,0:T(8,128)S(1)} %broadcast_bitcast_fusion.3, f32[1,4,8,128]{3,2,1,0:T(8,128)S(1)} %get-tuple-element.16, ...), kind=kOutput, calls=%fused_computation.14 | convolution fusion | flops 8425472 | bytes 2195456 | tf_op jit(solution)/shard_map/dot_general | solution.py:175
  28.9 1.2 %collective-permute-done.7 = bf16[4,512]{1,0:T(4,128)(2,1)S(1)} collective-permute-done((bf16[4,512]{1,0:T(4,128)(2,1)S(1)}, bf16[4,512]{1,0:T(4,128)(2,1)S(1)}, u32[]{:S(2)}, u32[]{:S(2)}) %collective-permute-start.7) | collective-permute-done | bytes 4128 | tf_op jit(solution)/shard_map/ppermute | solution.py:180
  30.1 0.7 %broadcast_in_dim.5 = bf16[32,4,512]{2,1,0:T(4,128)(2,1)} broadcast(bf16[4,512]{1,0:T(4,128)(2,1)S(1)} %add_convert_fusion.2), dimensions={1,2} | broadcast | bytes 135168 | tf_op jit(solution)/shard_map/broadcast_in_dim | solution.py:185
  30.8 4.3 %all-to-all-start = ((bf16[32,4,512]{2,1,0:T(4,128)(2,1)}), bf16[32,4,512]{2,1,0:T(4,128)(2,1)S(1)}, u32[]{:S(2)}, u32[]{:S(2)}) async-start(bf16[32,4,512]{2,1,0:T(4,128)(2,1)} %broadcast_in_dim.5), calls=%async_computation | async-start | bytes 262144 | tf_op jit(solution)/shard_map/all_to_all | solution.py:184
  35.1 8.1 %all-to-all-done = bf16[32,4,512]{2,1,0:T(4,128)(2,1)S(1)} async-done(((bf16[32,4,512]{2,1,0:T(4,128)(2,1)}), bf16[32,4,512]{2,1,0:T(4,128)(2,1)S(1)}, u32[]{:S(2)}, u32[]{:S(2)}) %all-to-all-start) | async-done | bytes 131104 | tf_op jit(solution)/shard_map/all_to_all | solution.py:184
  43.7 4.9 %fusion.5 = bf16[4,4,8,512]{3,1,2,0:T(4,128)(2,1)S(1)} fusion(bf16[64,8,8,512]{3,2,1,0:T(8,128)(2,1)} %bitcast.322, bf16[4,8,4,512]{3,2,1,0:T(4,128)(2,1)S(1)} %bitcast.324, bf16[8,512,512,1]{2,1,0,3:T(8,128)(2,1)} %bitcast.323), kind=kOutput, calls=%fused_computation.7 | convolution fusion | flops 134307840 | bytes 8650752 | tf_op jit(solution)/shard_map/arf,fcd->acrd/dot_general | solution.py:200
  48.6 9.9 %all_to_all.10 = bf16[32,4,512]{2,1,0:T(4,128)(2,1)S(1)} all-to-all(bf16[32,4,512]{2,1,0:T(4,128)(2,1)S(1)} %bitcast.325), channel_id=1, replica_groups=mesh['dp'=4,'kv'=4,'tp'=2] {'dp','kv','tp'}, dimensions={0} | all-to-all | bytes 262144 | tf_op jit(solution)/shard_map/all_to_all | solution.py:207
  58.5 0.6 %add_convert_fusion.1 = bf16[4,512]{1,0:T(4,128)(2,1)} fusion(f32[4,512]{1,0:T(4,128)S(1)} %convert_reduce_fusion, bf16[4,512]{1,0:T(4,128)(2,1)S(1)} %add_convert_fusion.2), kind=kLoop, calls=%fused_computation.92 | loop fusion | flops 6144 | bytes 16384 | tf_op jit(solution)/shard_map/convert_element_type | solution.py:209
  (88 shorter events, 3.7 us)
Async XLA Ops:
  0.0 15.8 %copy-start = (bf16[4,2048,1,128]{3,1,2,0:T(8,128)(2,1)S(1)}, bf16[4,2048,1,128]{3,1,2,0:T(8,128)(2,1)}, u32[]{:S(2)}) copy-start(bf16[4,2048,1,128]{3,1,2,0:T(8,128)(2,1)} %param.18) | copy-start | bytes 6291460
  0.0 5.5 %copy-start.4 = (bf16[4,512]{1,0:T(4,128)(2,1)S(1)}, bf16[4,512]{1,0:T(4,128)(2,1)}, u32[]{:S(2)}) copy-start(bf16[4,512]{1,0:T(4,128)(2,1)} %param.13) | copy-start | bytes 12292
  0.0 5.5 %copy-start.2 = (bf16[1024,128]{1,0:T(8,128)(2,1)S(1)}, bf16[1024,128]{1,0:T(8,128)(2,1)}, u32[]{:S(2)}) copy-start(bf16[1024,128]{1,0:T(8,128)(2,1)} %param.17) | copy-start | bytes 786436
  0.0 5.7 %copy-start.3 = (bf16[1024,128]{1,0:T(8,128)(2,1)S(1)}, bf16[1024,128]{1,0:T(8,128)(2,1)}, u32[]{:S(2)}) copy-start(bf16[1024,128]{1,0:T(8,128)(2,1)} %param.16) | copy-start | bytes 786436
  0.0 2.6 %collective-permute-start = (bf16[4,512]{1,0:T(4,128)(2,1)}, bf16[4,512]{1,0:T(4,128)(2,1)S(1)}, u32[]{:S(2)}, u32[]{:S(2)}) collective-permute-start(bf16[4,512]{1,0:T(4,128)(2,1)} %param.13), channel_id=1, source_target_pairs={{0,1},{1,0},{2,3},{3,2},{4,5},{5,4},{6,7},{7,6},{8,9},{9,8},{10,11... | collective-permute-start | bytes 12296 | tf_op jit(solution)/shard_map/ppermute | solution.py:92
  5.9 6.7 %collective-permute-start.1 = (f32[4,1408]{1,0:T(4,128)S(1)}, f32[4,1408]{1,0:T(4,128)S(1)}, u32[]{:S(2)}, u32[]{:S(2)}) collective-permute-start(f32[4,1408]{1,0:T(4,128)S(1)} %pad_maximum_fusion), channel_id=1, source_target_pairs={{0,2},{2,4},{4,6},{6,0},{1,3},{3,5},{5,7},{7,1},{8,10},{10,12},{12... | collective-permute-start | bytes 67592 | tf_op jit(solution)/shard_map/ppermute | solution.py:23
  8.7 4.7 %collective-permute-start.2 = (f32[4,1408]{1,0:T(4,128)S(1)}, f32[4,1408]{1,0:T(4,128)S(1)}, u32[]{:S(2)}, u32[]{:S(2)}) collective-permute-start(f32[4,1408]{1,0:T(4,128)S(1)} %pad_maximum_fusion), channel_id=1, source_target_pairs={{0,4},{2,6},{4,0},{6,2},{1,5},{3,7},{5,1},{7,3},{8,12},{10,14},{12... | collective-permute-start | bytes 67592 | tf_op jit(solution)/shard_map/ppermute | solution.py:23
  11.3 3.8 %collective-permute-start.3 = (f32[4,1408]{1,0:T(4,128)S(1)}, f32[4,1408]{1,0:T(4,128)S(1)}, u32[]{:S(2)}, u32[]{:S(2)}) collective-permute-start(f32[4,1408]{1,0:T(4,128)S(1)} %pad_maximum_fusion), channel_id=1, source_target_pairs={{0,6},{2,0},{4,2},{6,4},{1,7},{3,1},{5,3},{7,5},{8,14},{10,8},{12,... | collective-permute-start | bytes 67592 | tf_op jit(solution)/shard_map/ppermute | solution.py:23
  15.5 1.6 %copy-start.1 = (bf16[4,2048,1,128]{3,1,2,0:T(8,128)(2,1)S(1)}, bf16[4,2048,1,128]{3,1,2,0:T(8,128)(2,1)}, u32[]{:S(2)}) copy-start(bf16[4,2048,1,128]{3,1,2,0:T(8,128)(2,1)} %param.19) | copy-start | bytes 6291460
  17.1 9.5 %copy-start.6 = (f32[8]{0:T(128)S(1)}, f32[8]{0:T(128)}, u32[]{:S(2)}) copy-start(f32[8]{0:T(128)} %param.20) | copy-start | bytes 100
  17.5 17.5 %copy-start.5 = (bf16[4096]{0:T(1024)(128)(2,1)S(1)}, bf16[4096]{0:T(1024)(128)(2,1)}, u32[]{:S(2)}) copy-start(bf16[4096]{0:T(1024)(128)(2,1)} %param.23) | copy-start | bytes 24580
  18.0 5.7 %collective-permute-start.4 = (bf16[80,128]{1,0:T(8,128)(2,1)S(1)}, bf16[80,128]{1,0:T(8,128)(2,1)S(1)}, u32[]{:S(2)}, u32[]{:S(2)}) collective-permute-start(bf16[80,128]{1,0:T(8,128)(2,1)S(1)} %fusion.25), channel_id=1, source_target_pairs={{0,2},{2,4},{4,6},{6,0},{1,3},{3,5},{5,7},{7,1},{8,10},{10,12},{12... | collective-permute-start | bytes 61448 | tf_op jit(solution)/shard_map/ppermute | solution.py:23
  18.2 5.8 %collective-permute-start.5 = (bf16[80,128]{1,0:T(8,128)(2,1)S(1)}, bf16[80,128]{1,0:T(8,128)(2,1)S(1)}, u32[]{:S(2)}, u32[]{:S(2)}) collective-permute-start(bf16[80,128]{1,0:T(8,128)(2,1)S(1)} %fusion.25), channel_id=1, source_target_pairs={{0,4},{2,6},{4,0},{6,2},{1,5},{3,7},{5,1},{7,3},{8,12},{10,14},{12... | collective-permute-start | bytes 61448 | tf_op jit(solution)/shard_map/ppermute | solution.py:23
  21.8 3.8 %collective-permute-start.6 = (bf16[80,128]{1,0:T(8,128)(2,1)S(1)}, bf16[80,128]{1,0:T(8,128)(2,1)S(1)}, u32[]{:S(2)}, u32[]{:S(2)}) collective-permute-start(bf16[80,128]{1,0:T(8,128)(2,1)S(1)} %fusion.25), channel_id=1, source_target_pairs={{0,6},{2,0},{4,2},{6,4},{1,7},{3,1},{5,3},{7,5},{8,14},{10,8},{12,... | collective-permute-start | bytes 61448 | tf_op jit(solution)/shard_map/ppermute | solution.py:23
  28.8 1.2 %collective-permute-start.7 = (bf16[4,512]{1,0:T(4,128)(2,1)S(1)}, bf16[4,512]{1,0:T(4,128)(2,1)S(1)}, u32[]{:S(2)}, u32[]{:S(2)}) collective-permute-start(bf16[4,512]{1,0:T(4,128)(2,1)S(1)} %broadcast_select_fusion), channel_id=1, source_target_pairs={{0,1},{1,0},{2,3},{3,2},{4,5},{5,4},{6,7},{7,6},{8,9},{9,8},{10,11... | collective-permute-start | bytes 12296 | tf_op jit(solution)/shard_map/ppermute | solution.py:180
  30.8 12.4 %all-to-all-start = ((bf16[32,4,512]{2,1,0:T(4,128)(2,1)}), bf16[32,4,512]{2,1,0:T(4,128)(2,1)S(1)}, u32[]{:S(2)}, u32[]{:S(2)}) async-start(bf16[32,4,512]{2,1,0:T(4,128)(2,1)} %broadcast_in_dim.5), calls=%async_computation | async-start | bytes 262144 | tf_op jit(solution)/shard_map/all_to_all | solution.py:184

commit v2 on v0

v2 whole, which is shorter than its diff:
```python
import functools
import numpy as np
import jax
import jax.numpy as jnp
from jax import lax
from jax.experimental import pallas as pl
from jax.experimental.pallas import tpu as pltpu
from jax.sharding import PartitionSpec as P

D = 4096
HD = 64
VD = 128
EPS = 1e-06
THETA = 500000.0
OUT_SCALE = 0.8
LANES = 128
FAR = -3e38

F32 = jnp.float32
BF = jnp.bfloat16
VMEM = pl.BlockSpec(memory_space=pltpu.VMEM)
SMEM = pl.BlockSpec(memory_space=pltpu.SMEM)
ANY = pl.BlockSpec(memory_space=pl.ANY)


def everyones(value, axis):
    count = lax.axis_size(axis)
    if count > 8:
        copies = jnp.broadcast_to(value[None], (count,) + value.shape)
        got = lax.all_to_all(copies, axis, 0, 0, tiled=True)
        return [got[k] for k in range(count)]
    got = [value]
    for step in reversed(range(1, count)):
        got.append(lax.ppermute(value, axis, [(i, i ^ step) for i in range(count)]))
    return got


def rounded(value):
    return value.astype(BF).astype(F32)


def flat_row(ref, first, count):
    return jnp.concatenate([ref[first + i : first + i + 1, :] for i in range(count)], axis=1)


def project_kernel(tokens, other, gain, w_query, w_key, w_value, out):
    first = lax.axis_index("tp") == 0
    own = tokens[...].astype(F32)
    their = other[...].astype(F32)
    slab = jnp.concatenate([jnp.where(first, own, their), jnp.where(first, their, own)], axis=1)
    gains = flat_row(gain[...].astype(F32), 0, gain.shape[0])
    scaled = (slab * gains).astype(BF)
    q = w_query.shape[1]
    k = q + w_key.shape[1]
    v = k + w_value.shape[1]
    out[:, :q] = jnp.dot(scaled, w_query[...], preferred_element_type=F32)
    out[:, q:k] = jnp.dot(scaled, w_key[...], preferred_element_type=F32)
    out[:, k:v] = jnp.dot(scaled, w_value[...], preferred_element_type=F32)
    square = jnp.sum(slab * slab, axis=1, keepdims=True)
    out[:, v:] = jnp.broadcast_to(square, (slab.shape[0], LANES))


def attend_kernel(heads, parts, table, keys, values, out):
    total = parts[0][...]
    for part in parts[1:]:
        total = total + part[...]
    rows = total.shape[0]
    width = total.shape[1] - LANES
    inverse = lax.rsqrt(total[:, width : width + 1] / D + EPS)
    total = total[:, :width] * inverse
    cosine = table[0:1, :]
    sine = table[1:2, :]
    lane = lax.broadcasted_iota(jnp.int32, (rows, LANES), 1)
    near = lax.rem(lane, HD) < HD // 2

    def rotate(piece):
        ahead = pltpu.roll(piece, LANES - HD // 2, 1)
        behind = pltpu.roll(piece, HD // 2, 1)
        return rounded(piece * cosine + jnp.where(near, ahead, behind) * sine)

    pieces = [total[:, h * LANES : (h + 1) * LANES] for h in range(heads + 2)]
    query = [rotate(piece) * (HD**-0.5) for piece in pieces[:heads]]
    new_key = rotate(pieces[heads])
    new_value = rounded(pieces[heads + 1])
    holds_new = lax.axis_index("kv") == 0
    lane_h = lax.broadcasted_iota(jnp.int32, (heads, LANES), 1)
    lane_s = lax.broadcasted_iota(jnp.int32, (2 * heads, LANES), 1)
    stats = jnp.zeros((2 * heads, LANES), F32)
    for r in range(rows):
        mine = jnp.concatenate([piece[r : r + 1, :] for piece in query], axis=0)
        wide = jnp.concatenate(
            [jnp.where(lane_h < HD, mine, 0.0), jnp.where(lane_h < HD, 0.0, mine)], axis=0
        )
        scores = lax.dot_general(
            wide.astype(BF), keys[r], (((1,), (1,)), ((), ())), preferred_element_type=F32
        )
        own = jnp.sum(wide * new_key[r : r + 1, :], axis=1, keepdims=True)
        own = jnp.where(holds_new, own, FAR)
        top = jnp.maximum(jnp.max(scores, axis=1, keepdims=True), own)
        weights = jnp.exp(scores - top)
        own_weight = jnp.exp(own - top)
        den = jnp.sum(weights, axis=1, keepdims=True) + own_weight
        num = jnp.dot(weights.astype(BF), values[r], preferred_element_type=F32)
        num = num + rounded(own_weight) * new_value[r : r + 1, :]
        out[2 * heads * r : 2 * heads * (r + 1), :] = num.astype(BF)
        for at, value in ((r, top), (rows + r, den)):
            high = rounded(value)
            middle = rounded(value - high)
            low = rounded(value - high - middle)
            for step, piece in enumerate((high, middle, low)):
                stats = jnp.where(lane_s == 2 * rows * step + at, piece, stats)
    out[2 * heads * rows :, :] = stats.astype(BF)


def merge_kernel(heads, rows, messages, lam, head_gain, w_out, mine, theirs):
    first = lax.axis_index("tp") == 0
    span = 2 * heads
    joined = []
    for message in messages:
        stats = message[span * rows :, :].astype(F32)
        middle = pltpu.roll(stats, LANES - 2 * rows, 1)
        low = pltpu.roll(stats, LANES - 4 * rows, 1)
        joined.append(stats + (middle + low))
    top = functools.reduce(jnp.maximum, joined)
    carried = [jnp.exp(part - top) for part in joined]
    den = sum(c * pltpu.roll(part, LANES - rows, 1) for c, part in zip(carried, joined))
    shares = [c / den for c in carried]
    sub = lax.broadcasted_iota(jnp.int32, (heads, LANES), 0)
    lams = jnp.zeros((heads, LANES), F32)
    for h in range(heads):
        lams = jnp.where(sub == h, lam[h], lams)
    gains = head_gain[...].astype(F32) * OUT_SCALE
    attended = []
    for r in range(rows):
        ratio = sum(
            share[:, r : r + 1] * message[span * r : span * (r + 1), :].astype(F32)
            for share, message in zip(shares, messages)
        )
        mix = ratio[:heads] - lams * ratio[heads:]
        spread = lax.rsqrt(jnp.mean(mix * mix, axis=1, keepdims=True) + EPS)
        attended.append(mix * spread * gains)
    wide = jnp.concatenate(
        [
            jnp.concatenate([part[h : h + 1, :] for part in attended], axis=0)
            for h in range(heads)
        ],
        axis=1,
    )
    branch = jnp.dot(wide.astype(BF), w_out[...], preferred_element_type=F32)
    half = branch.shape[1] // 2
    mine[...] = jnp.where(first, branch[:, :half], branch[:, half:]).astype(BF)
    theirs[...] = jnp.where(first, branch[:, half:], branch[:, :half]).astype(BF)


def hidden_kernel(tokens, mine, received, copies, hidden):
    branch = mine[...].astype(F32) + received[...].astype(F32)
    value = (tokens[...].astype(F32) + branch).astype(BF)
    hidden[...] = value
    for k in range(copies.shape[0]):
        copies[k] = value


def mixer_kernel(dps, everyone, gain, w_up, w_down, out):
    devices, rows, width = everyone.shape
    blocks = devices // dps
    grid = []
    square = jnp.zeros((dps * rows, 1), F32)
    for b in range(blocks):
        block = jnp.concatenate(
            [everyone[a * blocks + b].astype(F32) for a in range(dps)], axis=0
        )
        grid.append(block)
        square = square + jnp.sum(block * block, axis=1, keepdims=True)
    inverse = lax.rsqrt(square / D + EPS)
    per = width // LANES
    gains = gain[...].astype(F32)
    upward = jnp.zeros((dps * rows, w_up.shape[1]), F32)
    for b in range(blocks):
        normed = (grid[b] * inverse * flat_row(gains, b * per, per)).astype(BF)
        upward = upward + jnp.dot(
            normed, w_up[b * width : (b + 1) * width, :], preferred_element_type=F32
        )
    act = jnp.square(jnp.maximum(upward, 0.0)).astype(BF)
    for b in range(blocks):
        down = jnp.dot(
            act, w_down[:, b * width : (b + 1) * width], preferred_element_type=F32
        ).astype(BF)
        for a in range(dps):
            out[a * blocks + b] = down[a * rows : (a + 1) * rows, :]


def final_kernel(terms, hidden, out):
    total = terms[0].astype(F32)
    for k in range(1, terms.shape[0]):
        total = total + terms[k].astype(F32)
    out[...] = (hidden[...].astype(F32) + total).astype(BF)


def load_kernel(count, *refs):
    sources, held, sems = refs[:count], refs[count : 2 * count], refs[2 * count]
    copies = [
        pltpu.make_async_copy(source, target, sems.at[i])
        for i, (source, target) in enumerate(zip(sources, held))
    ]
    for copy in copies:
        copy.start()
    for copy in copies:
        copy.wait()


def loaded(*arrays):
    count = len(arrays)
    size = sum(array.size * array.dtype.itemsize for array in arrays)
    return pl.pallas_call(
        functools.partial(load_kernel, count),
        out_shape=[jax.ShapeDtypeStruct(array.shape, array.dtype) for array in arrays],
        in_specs=[pl.BlockSpec(memory_space=pltpu.HBM)] * count,
        out_specs=[VMEM] * count,
        scratch_shapes=[pltpu.SemaphoreType.DMA((count,))],
        compiler_params=pltpu.CompilerParams(vmem_limit_bytes=1 << 20),
        cost_estimate=pl.CostEstimate(flops=20 * size, bytes_accessed=size, transcendentals=0),
    )(*(pltpu.with_memory_space_constraint(array, pltpu.HBM) for array in arrays))


def tables(position):
    half = HD // 2
    angle = position * THETA ** (-np.arange(half, dtype=np.float64) * 2.0 / HD)
    cosine = np.tile(np.cos(angle), LANES // half)
    sine = np.tile(np.concatenate([-np.sin(angle), np.sin(angle)]), LANES // HD)
    rest = np.zeros((6, LANES))
    return jnp.asarray(np.concatenate([cosine[None], sine[None], rest]), F32)


def call(kernel, shapes, inputs, specs, mib):
    return pl.pallas_call(
        kernel,
        out_shape=shapes,
        in_specs=specs,
        out_specs=jax.tree.map(lambda _: VMEM, shapes),
        compiler_params=pltpu.CompilerParams(vmem_limit_bytes=mib << 20),
    )(*inputs)


def local(
    tokens,
    attn_gain,
    w_query,
    w_key,
    w_value,
    key_cache,
    value_cache,
    lam,
    head_gain,
    w_out,
    ffn_gain,
    w_up,
    w_down,
):
    rows, width = tokens.shape
    kv_count = lax.axis_size("kv")
    tp_count = lax.axis_size("tp")
    dp_count = lax.axis_size("dp")
    positions = key_cache.shape[1]
    heads = lam.shape[0]
    axes = ("dp", "kv", "tp")
    swap = [(0, 1), (1, 0)]
    assert tp_count == 2 and key_cache.shape[2] == 1 and 6 * rows <= LANES
    shape = jax.ShapeDtypeStruct

    other = lax.ppermute(tokens, "tp", swap)
    packed = w_query.shape[1] + w_key.shape[1] + w_value.shape[1] + LANES
    held, gain, query, key, value = loaded(
        tokens, attn_gain.reshape(-1, LANES), w_query, w_key, w_value
    )
    part = call(
        project_kernel,
        shape((rows, packed), F32),
        (held, other, gain, query, key, value),
        [VMEM] * 6,
        6,
    )
    parts = everyones(part, "kv")
    table, keys, values = loaded(
        tables(positions * kv_count),
        key_cache.reshape(rows, positions, 2 * HD),
        value_cache.reshape(rows, positions, VD),
    )
    count = len(parts)

    def attend(*refs):
        attend_kernel(heads, refs[:count], *refs[count:])

    message = call(
        attend,
        shape((2 * heads * (rows + 1), LANES), BF),
        (*parts, table, keys, values),
        [VMEM] * (count + 3),
        8,
    )
    messages = everyones(message, "kv")
    head_gain, w_out = loaded(head_gain.reshape(1, VD), w_out)

    def merge(*refs):
        merge_kernel(heads, rows, refs[:count], *refs[count:])

    mine, theirs = call(
        merge,
        (shape((rows, width), BF), shape((rows, width), BF)),
        (*messages, lam, head_gain, w_out),
        [VMEM] * count + [SMEM, VMEM, VMEM],
        5,
    )
    received = lax.ppermute(theirs, "tp", swap)
    devices = dp_count * kv_count * tp_count
    copies, hidden = call(
        hidden_kernel,
        (shape((devices, rows, width), BF), shape((rows, width), BF)),
        (held, mine, received),
        [VMEM] * 3,
        2,
    )
    everyone = lax.all_to_all(copies, axes, 0, 0, tiled=True)
    term = call(
        functools.partial(mixer_kernel, dp_count),
        shape((devices, rows, width), BF),
        (everyone, ffn_gain.reshape(-1, LANES), w_up, w_down),
        [VMEM] * 4,
        12,
    )
    terms = lax.all_to_all(term, axes, 0, 0, tiled=True)
    return call(final_kernel, shape((rows, width), BF), (terms, hidden), [VMEM] * 2, 2)


def solution(mesh):
    in_specs = (
        P("dp", ("kv", "tp")),
        P("kv"),
        P("kv", "tp"),
        P("kv", "tp"),
        P("kv", "tp"),
        P("dp", "kv", "tp", None),
        P("dp", "kv", "tp", None),
        P("tp"),
        P(),
        P("tp", "kv"),
        P(),
        P(None, ("dp", "kv", "tp")),
        P(("dp", "kv", "tp"), None),
    )
    out_specs = P("dp", ("kv", "tp"))
    return jax.shard_map(local, mesh=mesh, in_specs=in_specs, out_specs=out_specs, check_vma=False)
```

time: 270 us -> 47.4 us (0.18)
  waiting for transfers between devices: 130 us -> 3.67 us
  blocking collectives: 102 us -> 21.9 us
  between operations: 13.6 us -> 0.07 us
  matrix products: 11.9 us -> 0 us
  Pallas kernels: 0 us -> 11.3 us
  starting transfers between devices: 0.04 us -> 10.2 us
  local copies, waits for them, and re-layouts: 8.44 us -> 0.01 us
  other arithmetic: 4.21 us -> 0 us
    unnamed x4 -> x0, waiting for transfers between devices: 130 us -> none
    all_gather x5 -> x0, blocking collectives: 81.4 us -> none  [the longest x1 42.2 us: local(): lax.all_gather(hidden[None], ('dp', 'kv', 'tp'), axis=0, tiled=True)]
    all_to_all x0 -> x2, blocking collectives: none -> 21.9 us  [the longest x1 12 us: local(): everyone = lax.all_to_all(copies, axes, 0, 0, tiled=True)]
    psum x1 -> x0, blocking collectives: 20.6 us -> none  [local(): lax.psum((part_q, part_k, part_v, local_sq), 'kv')]
    dot_general x8 -> x0, matrix products: 11.9 us -> none  [the longest x1 4.87 us: local(): jnp.einsum('arf,fcd->acrd', act, w_down.reshape(w_down.shape[0], blocks,...]
    pallas_call x0 -> x9, Pallas kernels: none -> 11.3 us  [the longest x3 5.77 us: loaded(): pl.pallas_call(functools.partial(load_kernel, count), out_shape=[jax.Shap...]
    ppermute x0 -> x8, starting transfers between devices: none -> 10.2 us  [the longest x6 9.74 us: everyones(): got.append(lax.ppermute(value, axis, [(i, i ^ step) for i in range(count)]))]
    unnamed x22 -> x8, local copies, waits for them, and re-layouts: 6.33 us -> 0.01 us
  transfers between devices with their start and end apart: 2 -> 8, of which waited for: 2 -> 3; matrix products, arithmetic and copies ran while one was open for 0% -> 0% of each run, Pallas kernels for 0% -> 12%
where the time goes in v2:
time: 47.4 us; the launch traced here: 47.2 us
  blocking collectives  21.9 us (46%)
  Pallas kernels  11.3 us (24%)
  starting transfers between devices  10.2 us (22%)
  waiting for transfers between devices  3.67 us (8%)
    all_to_all x1, blocking collectives, local(): everyone = lax.all_to_all(copies, axes, 0, 0, tiled=True)  12 us
    all_to_all x1, blocking collectives, local(): terms = lax.all_to_all(term, axes, 0, 0, tiled=True)  9.86 us
    ppermute x6, starting transfers between devices, everyones(): got.append(lax.ppermute(value, axis, [(i, i ^ step) for i in range(count)]))  9.74 us
    pallas_call x3, Pallas kernels, loaded(): pl.pallas_call(functools.partial(load_kernel, count), out_shape=[jax.Shap...  5.77 us
    pallas_call x6, Pallas kernels, call(): pl.pallas_call(kernel, out_shape=shapes, in_specs=specs, out_specs=jax.tr...  5.56 us
    ppermute x6, waiting for transfers between devices, everyones(): got.append(lax.ppermute(value, axis, [(i, i ^ step) for i in range(count)]))  2.5 us
    ppermute x1, waiting for transfers between devices, local(): received = lax.ppermute(theirs, 'tp', swap)  1.17 us
  transfers between devices with their start and end apart: 8, of which 3 were waited for; matrix products, arithmetic and copies ran while one was open for 0% of the time, Pallas kernels for 12%

profile of v2, /device:TPU:0, one launch (start us, length us, event | category | flops | bytes accessed | tf_op | source)
XLA Modules:
  0.0 47.2 jit_solution(8730178870816546835)
XLA Ops:
  0.0 0.5 %collective-permute-start = (bf16[4,512]{1,0:T(4,128)(2,1)}, bf16[4,512]{1,0:T(4,128)(2,1)S(1)}, u32[]{:S(2)}, u32[]{:S(2)}) collective-permute-start(bf16[4,512]{1,0:T(4,128)(2,1)} %refs_0_.2), channel_id=1, source_target_pairs={{0,1},{1,0},{2,3},{3,2},{4,5},{5,4},{6,7},{7,6},{8,9},{9,8},{10,11... | collective-permute-start | bytes 12296 | tf_op jit(solution)/shard_map/ppermute | solution.py:270
  0.5 1.7 %shard_map.136 = (bf16[4,512]{1,0:T(4,128)(2,1)S(1)}, bf16[8,128]{1,0:T(8,128)(2,1)S(1)}, bf16[1024,1024]{1,0:T(8,128)(2,1)S(1)}, bf16[1024,128]{1,0:T(8,128)(2,1)S(1)}, bf16[1024,128]{1,0:T(8,128)(2,1)S(1)}) custom-call(bf16[4,512]{1,0:T(4,128)(2,1)} %refs_0_.2, bf16[8,128]{1,0:T(8,128)(2,1)} %bitcast.8, bf16[1024,1024]{1,0:T(8,128)(2,1)} %refs_2_.1, ...), custom_call_target="tpu_custom_call" | custom-call | flops 52551680 | bytes 2627584 | tf_op jit(solution)/shard_map/pallas_call | solution.py:214
  2.2 0.0 collective-permute-done.other
  2.2 0.4 shard_map.137.refs_0_
  2.7 4.6 %collective-permute-start.1 = (f32[4,1408]{1,0:T(4,128)S(1)}, f32[4,1408]{1,0:T(4,128)S(1)}, u32[]{:S(2)}, u32[]{:S(2)}) collective-permute-start(f32[4,1408]{1,0:T(4,128)S(1)} %shard_map.137.refs_0_), channel_id=1, source_target_pairs={{0,6},{2,4},{4,2},{6,0},{1,7},{3,5},{5,3},{7,1},{8,14},{10,12},{12... | collective-permute-start | bytes 67592 | tf_op jit(solution)/shard_map/ppermute | solution.py:34
  7.3 0.0 collective-permute-start.2
  7.3 0.6 %collective-permute-start.3 = (f32[4,1408]{1,0:T(4,128)S(1)}, f32[4,1408]{1,0:T(4,128)S(1)}, u32[]{:S(2)}, u32[]{:S(2)}) collective-permute-start(f32[4,1408]{1,0:T(4,128)S(1)} %shard_map.137.refs_0_), channel_id=1, source_target_pairs={{0,2},{2,0},{4,6},{6,4},{1,3},{3,1},{5,7},{7,5},{8,10},{10,8},{12,... | collective-permute-start | bytes 67592 | tf_op jit(solution)/shard_map/ppermute | solution.py:34
  8.0 2.3 %shard_map.138 = (f32[8,128]{1,0:T(8,128)S(1)}, bf16[4,2048,128]{2,1,0:T(8,128)(2,1)S(1)}, bf16[4,2048,128]{2,1,0:T(8,128)(2,1)S(1)}) custom-call(f32[8,128]{1,0:T(8,128)} %constant.2.clone.refs_0_, bf16[4,2048,128]{2,1,0:T(8,128)(2,1)} %bitcast.6, bf16[4,2048,128]{2,1,0:T(8,128)(2,1)} %bitcast.7), custom_call_target="tpu_custom_call" | custom-call | flops 83968000 | bytes 4198400 | tf_op jit(solution)/shard_map/pallas_call | solution.py:214
  10.2 0.0 collective-permute-done.1.refs_1_
  10.3 1.8 %collective-permute-done.2.refs_2_ = f32[4,1408]{1,0:T(4,128)S(1)} collective-permute-done((f32[4,1408]{1,0:T(4,128)S(1)}, f32[4,1408]{1,0:T(4,128)S(1)}, u32[]{:S(2)}, u32[]{:S(2)}) %collective-permute-start.2) | collective-permute-done | bytes 22560 | tf_op jit(solution)/shard_map/ppermute | solution.py:34
  12.0 0.0 collective-permute-done.3.refs_3_
  12.0 0.0 copy-start.1
  12.0 1.8 %shard_map.139.refs_0_ = bf16[80,128]{1,0:T(8,128)(2,1)S(1)} custom-call(f32[4,1408]{1,0:T(4,128)S(1)} %shard_map.137.refs_0_, f32[4,1408]{1,0:T(4,128)S(1)} %collective-permute-done.1.refs_1_, f32[4,1408]{1,0:T(4,128)S(1)} %collective-permute-done.2.refs_2_, f32[4,1408]{1,0:T(4,128)S(1)} %collective-permute-done.3.refs_3_, ...), custom_call_target="tpu_custom_call" | custom-call | tf_op jit(solution)/shard_map/pallas_call | solution.py:235
  13.9 0.0 copy-start.3
  13.9 2.1 %collective-permute-start.4 = (bf16[80,128]{1,0:T(8,128)(2,1)S(1)}, bf16[80,128]{1,0:T(8,128)(2,1)S(1)}, u32[]{:S(2)}, u32[]{:S(2)}) collective-permute-start(bf16[80,128]{1,0:T(8,128)(2,1)S(1)} %shard_map.139.refs_0_), channel_id=1, source_target_pairs={{0,6},{2,4},{4,2},{6,0},{1,7},{3,5},{5,3},{7,1},{8,14},{10,12},{12... | collective-permute-start | bytes 61448 | tf_op jit(solution)/shard_map/ppermute | solution.py:34
  15.9 0.1 collective-permute-start.5
  16.0 2.3 %collective-permute-start.6 = (bf16[80,128]{1,0:T(8,128)(2,1)S(1)}, bf16[80,128]{1,0:T(8,128)(2,1)S(1)}, u32[]{:S(2)}, u32[]{:S(2)}) collective-permute-start(bf16[80,128]{1,0:T(8,128)(2,1)S(1)} %shard_map.139.refs_0_), channel_id=1, source_target_pairs={{0,2},{2,0},{4,6},{6,4},{1,3},{3,1},{5,7},{7,5},{8,10},{10,8},{12,... | collective-permute-start | bytes 61448 | tf_op jit(solution)/shard_map/ppermute | solution.py:34
  18.3 1.8 %shard_map.140 = (bf16[1,128]{1,0:T(2,128)(2,1)S(1)}, bf16[1024,1024]{1,0:T(8,128)(2,1)S(1)}) custom-call(bf16[1,128]{1,0:T(2,128)(2,1)} %bitcast.9, bf16[1024,1024]{1,0:T(8,128)(2,1)} %refs_1_.1), custom_call_target="tpu_custom_call" | custom-call | flops 41948160 | bytes 2097408 | tf_op jit(solution)/shard_map/pallas_call | solution.py:214
  20.1 0.0 collective-permute-done.4.refs_1_
  20.1 0.7 %collective-permute-done.5.refs_2_ = bf16[80,128]{1,0:T(8,128)(2,1)S(1)} collective-permute-done((bf16[80,128]{1,0:T(8,128)(2,1)S(1)}, bf16[80,128]{1,0:T(8,128)(2,1)S(1)}, u32[]{:S(2)}, u32[]{:S(2)}) %collective-permute-start.5) | collective-permute-done | bytes 20512 | tf_op jit(solution)/shard_map/ppermute | solution.py:34
  20.8 0.0 collective-permute-done.6.refs_3_
  20.8 0.0 copy-done.3
  20.8 1.3 %shard_map.141 = (bf16[4,512]{1,0:T(4,128)(2,1)S(1)}, bf16[4,512]{1,0:T(4,128)(2,1)S(1)}) custom-call(bf16[80,128]{1,0:T(8,128)(2,1)S(1)} %shard_map.139.refs_0_, bf16[80,128]{1,0:T(8,128)(2,1)S(1)} %collective-permute-done.4.refs_1_, bf16[80,128]{1,0:T(8,128)(2,1)S(1)} %collective-permute-done.5.refs_2_, ...), custom_call_target="tpu_custom_call" | custom-call | tf_op jit(solution)/shard_map/pallas_call | solution.py:235
  22.1 0.0 collective-permute-start.7
  22.1 1.2 %collective-permute-done.7.received = bf16[4,512]{1,0:T(4,128)(2,1)S(1)} collective-permute-done((bf16[4,512]{1,0:T(4,128)(2,1)S(1)}, bf16[4,512]{1,0:T(4,128)(2,1)S(1)}, u32[]{:S(2)}, u32[]{:S(2)}) %collective-permute-start.7) | collective-permute-done | bytes 4128 | tf_op jit(solution)/shard_map/ppermute | solution.py:313
  23.3 12.0 %all_to_all.10.everyone = bf16[32,4,512]{2,1,0:T(4,128)(2,1)S(1)} all-to-all(bf16[32,4,512]{2,1,0:T(4,128)(2,1)S(1)} %get-tuple-element.31), channel_id=1, replica_groups=mesh['dp'=4,'kv'=4,'tp'=2] {'dp','kv','tp'}, dimensions={0} | all-to-all | bytes 262144 | tf_op jit(solution)/shard_map/all_to_all | solution.py:322
  35.3 0.0 copy-done.1
  35.3 0.0 copy-done
  35.4 0.0 copy-done.2
  35.4 1.4 %shard_map.143 = bf16[32,4,512]{2,1,0:T(4,128)(2,1)S(1)} custom-call(bf16[32,4,512]{2,1,0:T(4,128)(2,1)S(1)} %all_to_all.10.everyone, bf16[32,128]{1,0:T(8,128)(2,1)S(1)} %bitcast.5, bf16[4096,512]{1,0:T(8,128)(2,1)S(1)} %copy-done, bf16[512,4096]{1,0:T(8,128)(2,1)S(1)} %copy-done.1), custom_call_target="tpu_custom_call" | custom-call | tf_op jit(solution)/shard_map/pallas_call | solution.py:235
  36.7 9.9 %all_to_all.11.terms = bf16[32,4,512]{2,1,0:T(4,128)(2,1)S(1)} all-to-all(bf16[32,4,512]{2,1,0:T(4,128)(2,1)S(1)} %shard_map.143), channel_id=1, replica_groups=mesh['dp'=4,'kv'=4,'tp'=2] {'dp','kv','tp'}, dimensions={0} | all-to-all | bytes 262144 | tf_op jit(solution)/shard_map/all_to_all | solution.py:330
  46.6 0.6 %shard_map.144 = bf16[4,512]{1,0:T(4,128)(2,1)} custom-call(bf16[32,4,512]{2,1,0:T(4,128)(2,1)S(1)} %all_to_all.11.terms, bf16[4,512]{1,0:T(4,128)(2,1)S(1)} %get-tuple-element.32.hidden), custom_call_target="tpu_custom_call" | custom-call | tf_op jit(solution)/shard_map/pallas_call | solution.py:235
  (3 shorter events, 0.0 us)
Async XLA Ops:
  0.0 2.2 %collective-permute-start = (bf16[4,512]{1,0:T(4,128)(2,1)}, bf16[4,512]{1,0:T(4,128)(2,1)S(1)}, u32[]{:S(2)}, u32[]{:S(2)}) collective-permute-start(bf16[4,512]{1,0:T(4,128)(2,1)} %refs_0_.2), channel_id=1, source_target_pairs={{0,1},{1,0},{2,3},{3,2},{4,5},{5,4},{6,7},{7,6},{8,9},{9,8},{10,11... | collective-permute-start | bytes 12296 | tf_op jit(solution)/shard_map/ppermute | solution.py:270
  2.7 7.6 %collective-permute-start.1 = (f32[4,1408]{1,0:T(4,128)S(1)}, f32[4,1408]{1,0:T(4,128)S(1)}, u32[]{:S(2)}, u32[]{:S(2)}) collective-permute-start(f32[4,1408]{1,0:T(4,128)S(1)} %shard_map.137.refs_0_), channel_id=1, source_target_pairs={{0,6},{2,4},{4,2},{6,0},{1,7},{3,5},{5,3},{7,1},{8,14},{10,12},{12... | collective-permute-start | bytes 67592 | tf_op jit(solution)/shard_map/ppermute | solution.py:34
  7.3 4.7 %collective-permute-start.2 = (f32[4,1408]{1,0:T(4,128)S(1)}, f32[4,1408]{1,0:T(4,128)S(1)}, u32[]{:S(2)}, u32[]{:S(2)}) collective-permute-start(f32[4,1408]{1,0:T(4,128)S(1)} %shard_map.137.refs_0_), channel_id=1, source_target_pairs={{0,4},{2,6},{4,0},{6,2},{1,5},{3,7},{5,1},{7,3},{8,12},{10,14},{12... | collective-permute-start | bytes 67592 | tf_op jit(solution)/shard_map/ppermute | solution.py:34
  7.3 4.7 %collective-permute-start.3 = (f32[4,1408]{1,0:T(4,128)S(1)}, f32[4,1408]{1,0:T(4,128)S(1)}, u32[]{:S(2)}, u32[]{:S(2)}) collective-permute-start(f32[4,1408]{1,0:T(4,128)S(1)} %shard_map.137.refs_0_), channel_id=1, source_target_pairs={{0,2},{2,0},{4,6},{6,4},{1,3},{3,1},{5,7},{7,5},{8,10},{10,8},{12,... | collective-permute-start | bytes 67592 | tf_op jit(solution)/shard_map/ppermute | solution.py:34
  12.0 23.3 %copy-start.1 = (bf16[512,4096]{1,0:T(8,128)(2,1)S(1)}, bf16[512,4096]{1,0:T(8,128)(2,1)}, u32[]{:S(2)}) copy-start(bf16[512,4096]{1,0:T(8,128)(2,1)} %w_down.1) | copy-start | bytes 12582916
  13.9 7.0 %copy-start.3 = (f32[8]{0:T(128)S(1)}, f32[8]{0:T(128)}, u32[]{:S(2)}) copy-start(f32[8]{0:T(128)} %refs_4_.3) | copy-start | bytes 100
  13.9 6.2 %collective-permute-start.4 = (bf16[80,128]{1,0:T(8,128)(2,1)S(1)}, bf16[80,128]{1,0:T(8,128)(2,1)S(1)}, u32[]{:S(2)}, u32[]{:S(2)}) collective-permute-start(bf16[80,128]{1,0:T(8,128)(2,1)S(1)} %shard_map.139.refs_0_), channel_id=1, source_target_pairs={{0,6},{2,4},{4,2},{6,0},{1,7},{3,5},{5,3},{7,1},{8,14},{10,12},{12... | collective-permute-start | bytes 61448 | tf_op jit(solution)/shard_map/ppermute | solution.py:34
  15.9 4.9 %collective-permute-start.5 = (bf16[80,128]{1,0:T(8,128)(2,1)S(1)}, bf16[80,128]{1,0:T(8,128)(2,1)S(1)}, u32[]{:S(2)}, u32[]{:S(2)}) collective-permute-start(bf16[80,128]{1,0:T(8,128)(2,1)S(1)} %shard_map.139.refs_0_), channel_id=1, source_target_pairs={{0,4},{2,6},{4,0},{6,2},{1,5},{3,7},{5,1},{7,3},{8,12},{10,14},{12... | collective-permute-start | bytes 61448 | tf_op jit(solution)/shard_map/ppermute | solution.py:34
  16.0 4.8 %collective-permute-start.6 = (bf16[80,128]{1,0:T(8,128)(2,1)S(1)}, bf16[80,128]{1,0:T(8,128)(2,1)S(1)}, u32[]{:S(2)}, u32[]{:S(2)}) collective-permute-start(bf16[80,128]{1,0:T(8,128)(2,1)S(1)} %shard_map.139.refs_0_), channel_id=1, source_target_pairs={{0,2},{2,0},{4,6},{6,4},{1,3},{3,1},{5,7},{7,5},{8,10},{10,8},{12,... | collective-permute-start | bytes 61448 | tf_op jit(solution)/shard_map/ppermute | solution.py:34
  18.3 17.0 %copy-start = (bf16[4096,512]{1,0:T(8,128)(2,1)S(1)}, bf16[4096,512]{1,0:T(8,128)(2,1)}, u32[]{:S(2)}) copy-start(bf16[4096,512]{1,0:T(8,128)(2,1)} %w_up.1) | copy-start | bytes 12582916
  18.3 17.0 %copy-start.2 = (bf16[4096]{0:T(1024)(128)(2,1)S(1)}, bf16[4096]{0:T(1024)(128)(2,1)}, u32[]{:S(2)}) copy-start(bf16[4096]{0:T(1024)(128)(2,1)} %param.24) | copy-start | bytes 24580
  22.1 1.2 %collective-permute-start.7 = (bf16[4,512]{1,0:T(4,128)(2,1)S(1)}, bf16[4,512]{1,0:T(4,128)(2,1)S(1)}, u32[]{:S(2)}, u32[]{:S(2)}) collective-permute-start(bf16[4,512]{1,0:T(4,128)(2,1)S(1)} %get-tuple-element.30), channel_id=1, source_target_pairs={{0,1},{1,0},{2,3},{3,2},{4,5},{5,4},{6,7},{7,6},{8,9},{9,8},{10,11... | collective-permute-start | bytes 12296 | tf_op jit(solution)/shard_map/ppermute | solution.py:313

commit v3 on v2

v3 whole, which is shorter than its diff:
```python
import functools
import numpy as np
import jax
import jax.numpy as jnp
from jax import lax
from jax.experimental import pallas as pl
from jax.experimental.pallas import tpu as pltpu
from jax.sharding import PartitionSpec as P

D = 4096
HD = 64
VD = 128
EPS = 1e-06
THETA = 500000.0
OUT_SCALE = 0.8
LANES = 128
FAR = -3e38

F32 = jnp.float32
BF = jnp.bfloat16
VMEM = pl.BlockSpec(memory_space=pltpu.VMEM)
SMEM = pl.BlockSpec(memory_space=pltpu.SMEM)
ANY = pl.BlockSpec(memory_space=pl.ANY)


def rounds(count, first):
    if count == 4 and first:
        return ((1, 3, 0, 2), (3, 2, 1, 0), (2, 0, 3, 1))
    return [[(i + step) % count for i in range(count)] for step in reversed(range(1, count))]


def everyones(value, axis, first):
    count = lax.axis_size(axis)
    if count > 8:
        copies = jnp.broadcast_to(value[None], (count,) + value.shape)
        got = lax.all_to_all(copies, axis, 0, 0, tiled=True)
        return [got[k] for k in range(count)]
    got = [value]
    for pairs in rounds(count, first):
        got.append(lax.ppermute(value, axis, list(enumerate(pairs))))
    return got


def rounded(value):
    return value.astype(BF).astype(F32)


def flat_row(ref, first, count):
    return jnp.concatenate([ref[first + i : first + i + 1, :] for i in range(count)], axis=1)


def project_kernel(tokens, other, gain, w_query, w_key, w_value, out):
    first = lax.axis_index("tp") == 0
    own = tokens[...].astype(F32)
    their = other[...].astype(F32)
    slab = jnp.concatenate([jnp.where(first, own, their), jnp.where(first, their, own)], axis=1)
    gains = flat_row(gain[...].astype(F32), 0, gain.shape[0])
    scaled = (slab * gains).astype(BF)
    q = w_query.shape[1]
    k = q + w_key.shape[1]
    v = k + w_value.shape[1]
    out[:, :q] = jnp.dot(scaled, w_query[...], preferred_element_type=F32)
    out[:, q:k] = jnp.dot(scaled, w_key[...], preferred_element_type=F32)
    out[:, k:v] = jnp.dot(scaled, w_value[...], preferred_element_type=F32)
    square = jnp.sum(slab * slab, axis=1, keepdims=True)
    out[:, v:] = jnp.broadcast_to(square, (slab.shape[0], LANES))


def attend_kernel(heads, parts, table, keys, values, out, turn):
    total = parts[0][...]
    for part in parts[1:]:
        total = total + part[...]
    rows = total.shape[0]
    span = 2 * heads
    width = total.shape[1] - LANES
    inverse = lax.rsqrt(total[:, width : width + 1] / D + EPS)
    cosine = table[0:1, :]
    sine = table[1:2, :]
    lane = lax.broadcasted_iota(jnp.int32, (rows, LANES), 1)
    near = lax.rem(lane, HD) < HD // 2

    def rotate(piece):
        ahead = pltpu.roll(piece, LANES - HD // 2, 1)
        behind = pltpu.roll(piece, HD // 2, 1)
        return rounded(piece * cosine + jnp.where(near, ahead, behind) * sine)

    pieces = [total[:, h * LANES : (h + 1) * LANES] * inverse for h in range(heads + 2)]
    for h in range(heads):
        turn[h * rows : (h + 1) * rows, :] = rotate(pieces[h]) * (HD**-0.5)
    new_key = rotate(pieces[heads])
    new_value = rounded(pieces[heads + 1])
    holds_new = lax.axis_index("kv") == 0
    lane_h = lax.broadcasted_iota(jnp.int32, (heads, LANES), 1)
    lane_s = lax.broadcasted_iota(jnp.int32, (span, LANES), 1)
    wide = []
    for r in range(rows):
        mine = turn[pl.ds(r, heads, stride=rows), :]
        wide.append(
            jnp.concatenate(
                [jnp.where(lane_h < HD, mine, 0.0), jnp.where(lane_h < HD, 0.0, mine)], axis=0
            )
        )
    scores = [
        lax.dot_general(
            wide[r].astype(BF), keys[r], (((1,), (1,)), ((), ())), preferred_element_type=F32
        )
        for r in range(rows)
    ]
    own = [
        jnp.where(holds_new, jnp.sum(wide[r] * new_key[r : r + 1, :], axis=1, keepdims=True), FAR)
        for r in range(rows)
    ]
    top = [
        jnp.maximum(jnp.max(scores[r], axis=1, keepdims=True), own[r]) for r in range(rows)
    ]
    weights = [jnp.exp(scores[r] - top[r]) for r in range(rows)]
    own_weight = [jnp.exp(own[r] - top[r]) for r in range(rows)]
    num = [
        jnp.dot(weights[r].astype(BF), values[r], preferred_element_type=F32)
        for r in range(rows)
    ]
    den = [
        jnp.sum(weights[r], axis=1, keepdims=True) + own_weight[r] for r in range(rows)
    ]
    flat = jnp.zeros((span, LANES), F32)
    for r in range(rows):
        flat = jnp.where(lane_s == r, top[r], flat)
        flat = jnp.where(lane_s == rows + r, den[r], flat)
    high = rounded(flat)
    middle = rounded(flat - high)
    low = rounded(flat - high - middle)
    stats = high + pltpu.roll(middle, 2 * rows, 1) + pltpu.roll(low, 4 * rows, 1)
    out[span * rows :, :] = stats.astype(BF)
    for r in range(rows):
        value = num[r] + rounded(own_weight[r]) * new_value[r : r + 1, :]
        out[span * r : span * (r + 1), :] = value.astype(BF)


def merge_kernel(heads, rows, messages, lam, head_gain, w_out, mine, theirs, turn):
    first = lax.axis_index("tp") == 0
    span = 2 * heads
    joined = []
    for message in messages:
        stats = message[span * rows :, :].astype(F32)
        middle = pltpu.roll(stats, LANES - 2 * rows, 1)
        low = pltpu.roll(stats, LANES - 4 * rows, 1)
        joined.append(stats + (middle + low))
    top = functools.reduce(jnp.maximum, joined)
    carried = [jnp.exp(part - top) for part in joined]
    den = sum(c * pltpu.roll(part, LANES - rows, 1) for c, part in zip(carried, joined))
    shares = [c / den for c in carried]
    sub = lax.broadcasted_iota(jnp.int32, (heads, heads), 0)
    across = lax.broadcasted_iota(jnp.int32, (heads, heads), 1)
    lams = jnp.sum(jnp.where(sub == across, lam[...], 0.0), axis=1, keepdims=True)
    gains = head_gain[...].astype(F32) * OUT_SCALE
    mixes = []
    for r in range(rows):
        ratio = sum(
            share[:, r : r + 1] * message[span * r : span * (r + 1), :].astype(F32)
            for share, message in zip(shares, messages)
        )
        mixes.append(ratio[:heads] - lams * ratio[heads:])
    means = [jnp.mean(mix * mix, axis=1, keepdims=True) for mix in mixes]
    for r in range(rows):
        turn[r * heads : (r + 1) * heads, :] = mixes[r] * lax.rsqrt(means[r] + EPS) * gains
    wide = jnp.concatenate(
        [turn[pl.ds(h, rows, stride=heads), :] for h in range(heads)], axis=1
    )
    branch = jnp.dot(wide.astype(BF), w_out[...], preferred_element_type=F32)
    half = branch.shape[1] // 2
    mine[...] = jnp.where(first, branch[:, :half], branch[:, half:]).astype(BF)
    theirs[...] = jnp.where(first, branch[:, half:], branch[:, :half]).astype(BF)


def hidden_kernel(tokens, mine, received, copies, hidden):
    branch = mine[...].astype(F32) + received[...].astype(F32)
    value = (tokens[...].astype(F32) + branch).astype(BF)
    hidden[...] = value
    for k in range(copies.shape[0]):
        copies[k] = value


def mixer_kernel(dps, everyone, gain, w_up, w_down, out):
    devices, rows, width = everyone.shape
    blocks = devices // dps
    per = width // LANES
    gains = gain[...].astype(F32)
    square = jnp.zeros((dps * rows, width), F32)
    upward = jnp.zeros((dps * rows, w_up.shape[1]), F32)
    for b in range(blocks):
        block = jnp.concatenate(
            [everyone[a * blocks + b].astype(F32) for a in range(dps)], axis=0
        )
        square = square + block * block
        scaled = (block * flat_row(gains, b * per, per)).astype(BF)
        upward = upward + jnp.dot(
            scaled, w_up[b * width : (b + 1) * width, :], preferred_element_type=F32
        )
    inverse = lax.rsqrt(jnp.sum(square, axis=1, keepdims=True) / D + EPS)
    act = jnp.square(jnp.maximum(upward * inverse, 0.0)).astype(BF)
    for b in range(blocks):
        down = jnp.dot(
            act, w_down[:, b * width : (b + 1) * width], preferred_element_type=F32
        ).astype(BF)
        for a in range(dps):
            out[a * blocks + b] = down[a * rows : (a + 1) * rows, :]


def final_kernel(terms, hidden, out):
    total = terms[0].astype(F32)
    for k in range(1, terms.shape[0]):
        total = total + terms[k].astype(F32)
    out[...] = (hidden[...].astype(F32) + total).astype(BF)


def load_kernel(count, *refs):
    sources, held, sems = refs[:count], refs[count : 2 * count], refs[2 * count]
    copies = [
        pltpu.make_async_copy(source, target, sems.at[i])
        for i, (source, target) in enumerate(zip(sources, held))
    ]
    for copy in copies:
        copy.start()
    for copy in copies:
        copy.wait()


def loaded(*arrays):
    count = len(arrays)
    return pl.pallas_call(
        functools.partial(load_kernel, count),
        out_shape=[jax.ShapeDtypeStruct(array.shape, array.dtype) for array in arrays],
        in_specs=[pl.BlockSpec(memory_space=pltpu.HBM)] * count,
        out_specs=[VMEM] * count,
        scratch_shapes=[pltpu.SemaphoreType.DMA((count,))],
        compiler_params=pltpu.CompilerParams(vmem_limit_bytes=1 << 20),
        cost_estimate=pl.CostEstimate(
            flops=8 << 30, bytes_accessed=8 << 20, transcendentals=0
        ),
    )(*(pltpu.with_memory_space_constraint(array, pltpu.HBM) for array in arrays))


def tables(position):
    half = HD // 2
    angle = position * THETA ** (-np.arange(half, dtype=np.float64) * 2.0 / HD)
    cosine = np.tile(np.cos(angle), LANES // half)
    sine = np.tile(np.concatenate([-np.sin(angle), np.sin(angle)]), LANES // HD)
    rest = np.zeros((6, LANES))
    return jnp.asarray(np.concatenate([cosine[None], sine[None], rest]), F32)


def call(kernel, shapes, inputs, mib, cost=1, scratch=()):
    return pl.pallas_call(
        kernel,
        out_shape=shapes,
        in_specs=[VMEM] * len(inputs),
        out_specs=jax.tree.map(lambda _: VMEM, shapes),
        scratch_shapes=[pltpu.VMEM(shape, F32) for shape in scratch],
        compiler_params=pltpu.CompilerParams(vmem_limit_bytes=mib << 20),
        cost_estimate=pl.CostEstimate(
            flops=cost << 30, bytes_accessed=cost << 20, transcendentals=0
        ),
    )(*inputs)


def local(
    tokens,
    attn_gain,
    w_query,
    w_key,
    w_value,
    key_cache,
    value_cache,
    lam,
    head_gain,
    w_out,
    ffn_gain,
    w_up,
    w_down,
):
    rows, width = tokens.shape
    kv_count = lax.axis_size("kv")
    tp_count = lax.axis_size("tp")
    dp_count = lax.axis_size("dp")
    positions = key_cache.shape[1]
    heads = lam.shape[0]
    axes = ("dp", "kv", "tp")
    swap = [(0, 1), (1, 0)]
    assert tp_count == 2 and key_cache.shape[2] == 1 and 6 * rows <= LANES
    shape = jax.ShapeDtypeStruct

    other = lax.ppermute(tokens, "tp", swap)
    packed = w_query.shape[1] + w_key.shape[1] + w_value.shape[1] + LANES
    held, gain = loaded(tokens, attn_gain.reshape(-1, LANES))
    part = call(
        project_kernel,
        shape((rows, packed), F32),
        (held, other, gain, w_query, w_key, w_value),
        6,
        8,
    )
    parts = everyones(part, "kv", True)
    count = len(parts)

    def attend(*refs):
        attend_kernel(heads, refs[:count], *refs[count:])

    message = call(
        attend,
        shape((2 * heads * (rows + 1), LANES), BF),
        (
            *parts,
            tables(positions * kv_count),
            key_cache.reshape(rows, positions, 2 * HD),
            value_cache.reshape(rows, positions, VD),
        ),
        8,
        8,
        [(heads * rows, LANES)],
    )
    messages = everyones(message, "kv", False)

    def merge(*refs):
        merge_kernel(heads, rows, refs[:count], *refs[count:])

    mine, theirs = call(
        merge,
        (shape((rows, width), BF), shape((rows, width), BF)),
        (*messages, lam.reshape(1, heads), head_gain.reshape(1, VD), w_out),
        5,
        8,
        [(heads * rows, LANES)],
    )
    received = lax.ppermute(theirs, "tp", swap)
    devices = dp_count * kv_count * tp_count
    copies, hidden = call(
        hidden_kernel,
        (shape((devices, rows, width), BF), shape((rows, width), BF)),
        (held, mine, received),
        2,
    )
    everyone = lax.all_to_all(copies, axes, 0, 0, tiled=True)
    term = call(
        functools.partial(mixer_kernel, dp_count),
        shape((devices, rows, width), BF),
        (everyone, ffn_gain.reshape(-1, LANES), w_up, w_down),
        12,
    )
    terms = lax.all_to_all(term, axes, 0, 0, tiled=True)
    return call(final_kernel, shape((rows, width), BF), (terms, hidden), 2)


def solution(mesh):
    in_specs = (
        P("dp", ("kv", "tp")),
        P("kv"),
        P("kv", "tp"),
        P("kv", "tp"),
        P("kv", "tp"),
        P("dp", "kv", "tp", None),
        P("dp", "kv", "tp", None),
        P("tp"),
        P(),
        P("tp", "kv"),
        P(),
        P(None, ("dp", "kv", "tp")),
        P(("dp", "kv", "tp"), None),
    )
    out_specs = P("dp", ("kv", "tp"))
    return jax.shard_map(local, mesh=mesh, in_specs=in_specs, out_specs=out_specs, check_vma=False)
```

time: 47.4 us -> 47 us (level)
  Pallas kernels: 11.3 us -> 5.03 us
  waiting for transfers between devices: 3.67 us -> 8.23 us
  blocking collectives: 21.9 us -> 22.7 us
  local copies, waits for them, and re-layouts: 0.01 us -> 0.7 us
    pallas_call x3 -> x1, Pallas kernels: 5.77 us -> 0.86 us  [loaded(): pl.pallas_call(functools.partial(load_kernel, count), out_shape=[jax.Shap...]
    ppermute x6, waiting for transfers between devices: 2.5 us -> 6.9 us  [everyones(): got.append(lax.ppermute(value, axis, list(enumerate(pairs))))]
    pallas_call x6, Pallas kernels: 5.56 us -> 4.17 us  [call(): pl.pallas_call(kernel, out_shape=shapes, in_specs=[VMEM] * len(inputs), o...]
    all_to_all x1, blocking collectives: 12 us -> 12.8 us  [local(): everyone = lax.all_to_all(copies, axes, 0, 0, tiled=True)]
    unnamed x8 -> x24, local copies, waits for them, and re-layouts: 0.01 us -> 0.7 us
  transfers between devices with their start and end apart: 8 -> 8, of which waited for: 3 -> 6; matrix products, arithmetic and copies ran while one was open for 0% -> 0% of each run, Pallas kernels for 12% -> 2%
where the time goes in v3:
time: 47 us; the launch traced here: 46.8 us
  blocking collectives  22.7 us (48%)
  starting transfers between devices  10.1 us (21%)
  waiting for transfers between devices  8.23 us (18%)
  Pallas kernels  5.03 us (11%)
  local copies, waits for them, and re-layouts  0.7 us (1%)
    all_to_all x1, blocking collectives, local(): everyone = lax.all_to_all(copies, axes, 0, 0, tiled=True)  12.8 us
    all_to_all x1, blocking collectives, local(): terms = lax.all_to_all(term, axes, 0, 0, tiled=True)  9.86 us
    ppermute x6, starting transfers between devices, everyones(): got.append(lax.ppermute(value, axis, list(enumerate(pairs))))  9.63 us
    ppermute x6, waiting for transfers between devices, everyones(): got.append(lax.ppermute(value, axis, list(enumerate(pairs))))  6.9 us
    pallas_call x6, Pallas kernels, call(): pl.pallas_call(kernel, out_shape=shapes, in_specs=[VMEM] * len(inputs), o...  4.17 us
    ppermute x1, waiting for transfers between devices, local(): received = lax.ppermute(theirs, 'tp', swap)  1.17 us
  transfers between devices with their start and end apart: 8, of which 6 were waited for; matrix products, arithmetic and copies ran while one was open for 0% of the time, Pallas kernels for 2%

profile of v3, /device:TPU:0, one launch (start us, length us, event | category | flops | bytes accessed | tf_op | source)
XLA Modules:
  0.0 46.8 jit_solution(18374261622398773059)
XLA Ops:
  0.0 0.5 %collective-permute-start = (bf16[4,512]{1,0:T(4,128)(2,1)}, bf16[4,512]{1,0:T(4,128)(2,1)S(1)}, u32[]{:S(2)}, u32[]{:S(2)}) collective-permute-start(bf16[4,512]{1,0:T(4,128)(2,1)} %refs_0_.1), channel_id=1, source_target_pairs={{0,1},{1,0},{2,3},{3,2},{4,5},{5,4},{6,7},{7,6},{8,9},{9,8},{10,11... | collective-permute-start | bytes 12296 | tf_op jit(solution)/shard_map/ppermute | solution.py:292
  0.5 0.9 %shard_map.136 = (bf16[4,512]{1,0:T(4,128)(2,1)S(1)}, bf16[8,128]{1,0:T(8,128)(2,1)S(1)}) custom-call(bf16[4,512]{1,0:T(4,128)(2,1)} %refs_0_.1, bf16[8,128]{1,0:T(8,128)(2,1)} %bitcast.11), custom_call_target="tpu_custom_call" | custom-call | flops 8589934592 | bytes 8388608 | tf_op jit(solution)/shard_map/pallas_call | solution.py:230
  1.4 0.2 collective-permute-done.other
  1.5 0.6 %copy-done.3 = bf16[1024,1024]{1,0:T(8,128)(2,1)S(1)} copy-done((bf16[1024,1024]{1,0:T(8,128)(2,1)S(1)}, bf16[1024,1024]{1,0:T(8,128)(2,1)}, u32[]{:S(2)}) %copy-start.3) | copy-done | bytes 2097176
  2.1 0.0 copy-done.7
  2.1 0.1 copy-done.8
  2.2 0.4 shard_map.137.refs_0_
  2.6 3.6 %collective-permute-start.3 = (f32[4,1408]{1,0:T(4,128)S(1)}, f32[4,1408]{1,0:T(4,128)S(1)}, u32[]{:S(2)}, u32[]{:S(2)}) collective-permute-start(f32[4,1408]{1,0:T(4,128)S(1)} %shard_map.137.refs_0_), channel_id=1, source_target_pairs={{0,4},{2,0},{4,6},{6,2},{1,5},{3,1},{5,7},{7,3},{8,12},{10,8},{12,... | collective-permute-start | bytes 67592 | tf_op jit(solution)/shard_map/ppermute | solution.py:40
  6.3 1.3 %collective-permute-start.2 = (f32[4,1408]{1,0:T(4,128)S(1)}, f32[4,1408]{1,0:T(4,128)S(1)}, u32[]{:S(2)}, u32[]{:S(2)}) collective-permute-start(f32[4,1408]{1,0:T(4,128)S(1)} %shard_map.137.refs_0_), channel_id=1, source_target_pairs={{0,6},{2,4},{4,2},{6,0},{1,7},{3,5},{5,3},{7,1},{8,14},{10,12},{12... | collective-permute-start | bytes 67592 | tf_op jit(solution)/shard_map/ppermute | solution.py:40
  7.6 0.8 %collective-permute-start.1 = (f32[4,1408]{1,0:T(4,128)S(1)}, f32[4,1408]{1,0:T(4,128)S(1)}, u32[]{:S(2)}, u32[]{:S(2)}) collective-permute-start(f32[4,1408]{1,0:T(4,128)S(1)} %shard_map.137.refs_0_), channel_id=1, source_target_pairs={{0,2},{2,6},{4,0},{6,4},{1,3},{3,7},{5,1},{7,5},{8,10},{10,14},{12... | collective-permute-start | bytes 67592 | tf_op jit(solution)/shard_map/ppermute | solution.py:40
  8.4 0.0 collective-permute-done.3.refs_3_
  8.4 3.5 %collective-permute-done.2.refs_2_ = f32[4,1408]{1,0:T(4,128)S(1)} collective-permute-done((f32[4,1408]{1,0:T(4,128)S(1)}, f32[4,1408]{1,0:T(4,128)S(1)}, u32[]{:S(2)}, u32[]{:S(2)}) %collective-permute-start.2) | collective-permute-done | bytes 22560 | tf_op jit(solution)/shard_map/ppermute | solution.py:40
  11.9 0.4 collective-permute-done.1.refs_1_
  12.3 0.0 copy-done.4
  12.3 0.0 copy-start.6
  12.3 0.0 copy-start.9
  12.3 0.0 copy-start.10
  12.4 1.1 %shard_map.138.refs_0_ = bf16[80,128]{1,0:T(8,128)(2,1)S(1)} custom-call(f32[4,1408]{1,0:T(4,128)S(1)} %shard_map.137.refs_0_, f32[4,1408]{1,0:T(4,128)S(1)} %collective-permute-done.1.refs_1_, f32[4,1408]{1,0:T(4,128)S(1)} %collective-permute-done.2.refs_2_, f32[4,1408]{1,0:T(4,128)S(1)} %collective-permute-done.3.refs_3_, f32[8,128]{1,0:T(8,128)S(1)} %copy-done.11, ...), custom_call_target="tpu_custom_call" | custom-call | flops 8589934592 | bytes 8388608 | tf_op jit(solution)/shard_map/pallas_call | solution.py:253
  13.4 0.1 collective-permute-start.6
  13.5 3.0 %collective-permute-start.5 = (bf16[80,128]{1,0:T(8,128)(2,1)S(1)}, bf16[80,128]{1,0:T(8,128)(2,1)S(1)}, u32[]{:S(2)}, u32[]{:S(2)}) collective-permute-start(bf16[80,128]{1,0:T(8,128)(2,1)S(1)} %shard_map.138.refs_0_), channel_id=1, source_target_pairs={{0,4},{2,6},{4,0},{6,2},{1,5},{3,7},{5,1},{7,3},{8,12},{10,14},{12... | collective-permute-start | bytes 61448 | tf_op jit(solution)/shard_map/ppermute | solution.py:40
  16.5 0.8 %collective-permute-start.4 = (bf16[80,128]{1,0:T(8,128)(2,1)S(1)}, bf16[80,128]{1,0:T(8,128)(2,1)S(1)}, u32[]{:S(2)}, u32[]{:S(2)}) collective-permute-start(bf16[80,128]{1,0:T(8,128)(2,1)S(1)} %shard_map.138.refs_0_), channel_id=1, source_target_pairs={{0,6},{2,0},{4,2},{6,4},{1,7},{3,1},{5,3},{7,5},{8,14},{10,8},{12,... | collective-permute-start | bytes 61448 | tf_op jit(solution)/shard_map/ppermute | solution.py:40
  17.3 1.8 %collective-permute-done.6.refs_3_ = bf16[80,128]{1,0:T(8,128)(2,1)S(1)} collective-permute-done((bf16[80,128]{1,0:T(8,128)(2,1)S(1)}, bf16[80,128]{1,0:T(8,128)(2,1)S(1)}, u32[]{:S(2)}, u32[]{:S(2)}) %collective-permute-start.6) | collective-permute-done | bytes 20512 | tf_op jit(solution)/shard_map/ppermute | solution.py:40
  19.1 0.0 collective-permute-done.5.refs_2_
  19.1 1.2 %collective-permute-done.4.refs_1_ = bf16[80,128]{1,0:T(8,128)(2,1)S(1)} collective-permute-done((bf16[80,128]{1,0:T(8,128)(2,1)S(1)}, bf16[80,128]{1,0:T(8,128)(2,1)S(1)}, u32[]{:S(2)}, u32[]{:S(2)}) %collective-permute-start.4) | collective-permute-done | bytes 20512 | tf_op jit(solution)/shard_map/ppermute | solution.py:40
  20.3 0.0 copy-start.1
  20.3 0.7 %shard_map.139 = (bf16[4,512]{1,0:T(4,128)(2,1)S(1)}, bf16[4,512]{1,0:T(4,128)(2,1)S(1)}) custom-call(bf16[80,128]{1,0:T(8,128)(2,1)S(1)} %shard_map.138.refs_0_, bf16[80,128]{1,0:T(8,128)(2,1)S(1)} %collective-permute-done.4.refs_1_, bf16[80,128]{1,0:T(8,128)(2,1)S(1)} %collective-permute-done.5.refs_2_, ...), custom_call_target="tpu_custom_call" | custom-call | flops 8589934592 | bytes 8388608 | tf_op jit(solution)/shard_map/pallas_call | solution.py:253
  21.1 0.0 collective-permute-start.7
  21.1 1.2 %collective-permute-done.7.received = bf16[4,512]{1,0:T(4,128)(2,1)S(1)} collective-permute-done((bf16[4,512]{1,0:T(4,128)(2,1)S(1)}, bf16[4,512]{1,0:T(4,128)(2,1)S(1)}, u32[]{:S(2)}, u32[]{:S(2)}) %collective-permute-start.7) | collective-permute-done | bytes 4128 | tf_op jit(solution)/shard_map/ppermute | solution.py:334
  22.3 12.8 %all_to_all.10.everyone = bf16[32,4,512]{2,1,0:T(4,128)(2,1)S(1)} all-to-all(bf16[32,4,512]{2,1,0:T(4,128)(2,1)S(1)} %get-tuple-element.15), channel_id=1, replica_groups=mesh['dp'=4,'kv'=4,'tp'=2] {'dp','kv','tp'}, dimensions={0} | all-to-all | bytes 262144 | tf_op jit(solution)/shard_map/all_to_all | solution.py:342
  35.1 1.3 %shard_map.141 = bf16[32,4,512]{2,1,0:T(4,128)(2,1)S(1)} custom-call(bf16[32,4,512]{2,1,0:T(4,128)(2,1)S(1)} %all_to_all.10.everyone, bf16[32,128]{1,0:T(8,128)(2,1)S(1)} %bitcast.6, bf16[4096,512]{1,0:T(8,128)(2,1)S(1)} %copy-done, bf16[512,4096]{1,0:T(8,128)(2,1)S(1)} %copy-done.1), custom_call_target="tpu_custom_call" | custom-call | flops 1073741824 | bytes 1048576 | tf_op jit(solution)/shard_map/pallas_call | solution.py:253
  36.3 9.9 %all_to_all.11.terms = bf16[32,4,512]{2,1,0:T(4,128)(2,1)S(1)} all-to-all(bf16[32,4,512]{2,1,0:T(4,128)(2,1)S(1)} %shard_map.141), channel_id=1, replica_groups=mesh['dp'=4,'kv'=4,'tp'=2] {'dp','kv','tp'}, dimensions={0} | all-to-all | bytes 262144 | tf_op jit(solution)/shard_map/all_to_all | solution.py:349
  46.2 0.6 %shard_map.142 = bf16[4,512]{1,0:T(4,128)(2,1)} custom-call(bf16[32,4,512]{2,1,0:T(4,128)(2,1)S(1)} %all_to_all.11.terms, bf16[4,512]{1,0:T(4,128)(2,1)S(1)} %get-tuple-element.16.hidden), custom_call_target="tpu_custom_call" | custom-call | flops 1073741824 | bytes 1048576 | tf_op jit(solution)/shard_map/pallas_call | solution.py:253
  (17 shorter events, 0.0 us)
Async XLA Ops:
  0.0 1.5 %collective-permute-start = (bf16[4,512]{1,0:T(4,128)(2,1)}, bf16[4,512]{1,0:T(4,128)(2,1)S(1)}, u32[]{:S(2)}, u32[]{:S(2)}) collective-permute-start(bf16[4,512]{1,0:T(4,128)(2,1)} %refs_0_.1), channel_id=1, source_target_pairs={{0,1},{1,0},{2,3},{3,2},{4,5},{5,4},{6,7},{7,6},{8,9},{9,8},{10,11... | collective-permute-start | bytes 12296 | tf_op jit(solution)/shard_map/ppermute | solution.py:292
  0.5 1.6 %copy-start.3 = (bf16[1024,1024]{1,0:T(8,128)(2,1)S(1)}, bf16[1024,1024]{1,0:T(8,128)(2,1)}, u32[]{:S(2)}) copy-start(bf16[1024,1024]{1,0:T(8,128)(2,1)} %w_query.1) | copy-start | bytes 6291460
  0.5 1.6 %copy-start.7 = (bf16[1024,128]{1,0:T(8,128)(2,1)S(1)}, bf16[1024,128]{1,0:T(8,128)(2,1)}, u32[]{:S(2)}) copy-start(bf16[1024,128]{1,0:T(8,128)(2,1)} %w_key.1) | copy-start | bytes 786436
  0.5 1.7 %copy-start.8 = (bf16[1024,128]{1,0:T(8,128)(2,1)S(1)}, bf16[1024,128]{1,0:T(8,128)(2,1)}, u32[]{:S(2)}) copy-start(bf16[1024,128]{1,0:T(8,128)(2,1)} %w_value.1) | copy-start | bytes 786436
  2.2 10.1 %copy-start.4 = (bf16[4,2048,1,128]{3,1,2,0:T(8,128)(2,1)S(1)}, bf16[4,2048,1,128]{3,1,2,0:T(8,128)(2,1)}, u32[]{:S(2)}) copy-start(bf16[4,2048,1,128]{3,1,2,0:T(8,128)(2,1)} %param.19) | copy-start | bytes 6291460
  2.2 10.1 %copy-start.5 = (bf16[4,2048,1,128]{3,1,2,0:T(8,128)(2,1)S(1)}, bf16[4,2048,1,128]{3,1,2,0:T(8,128)(2,1)}, u32[]{:S(2)}) copy-start(bf16[4,2048,1,128]{3,1,2,0:T(8,128)(2,1)} %param.20) | copy-start | bytes 6291460
  2.2 10.1 %copy-start.11 = (f32[8,128]{1,0:T(8,128)S(1)}, f32[8,128]{1,0:T(8,128)}, u32[]{:S(2)}) copy-start(f32[8,128]{1,0:T(8,128)} %constant.2.clone.refs_4_) | copy-start | bytes 12292
  2.6 5.8 %collective-permute-start.3 = (f32[4,1408]{1,0:T(4,128)S(1)}, f32[4,1408]{1,0:T(4,128)S(1)}, u32[]{:S(2)}, u32[]{:S(2)}) collective-permute-start(f32[4,1408]{1,0:T(4,128)S(1)} %shard_map.137.refs_0_), channel_id=1, source_target_pairs={{0,4},{2,0},{4,6},{6,2},{1,5},{3,1},{5,7},{7,3},{8,12},{10,8},{12,... | collective-permute-start | bytes 67592 | tf_op jit(solution)/shard_map/ppermute | solution.py:40
  6.3 5.6 %collective-permute-start.2 = (f32[4,1408]{1,0:T(4,128)S(1)}, f32[4,1408]{1,0:T(4,128)S(1)}, u32[]{:S(2)}, u32[]{:S(2)}) collective-permute-start(f32[4,1408]{1,0:T(4,128)S(1)} %shard_map.137.refs_0_), channel_id=1, source_target_pairs={{0,6},{2,4},{4,2},{6,0},{1,7},{3,5},{5,3},{7,1},{8,14},{10,12},{12... | collective-permute-start | bytes 67592 | tf_op jit(solution)/shard_map/ppermute | solution.py:40
  7.6 4.7 %collective-permute-start.1 = (f32[4,1408]{1,0:T(4,128)S(1)}, f32[4,1408]{1,0:T(4,128)S(1)}, u32[]{:S(2)}, u32[]{:S(2)}) collective-permute-start(f32[4,1408]{1,0:T(4,128)S(1)} %shard_map.137.refs_0_), channel_id=1, source_target_pairs={{0,2},{2,6},{4,0},{6,4},{1,3},{3,7},{5,1},{7,5},{8,10},{10,14},{12... | collective-permute-start | bytes 67592 | tf_op jit(solution)/shard_map/ppermute | solution.py:40
  12.3 8.0 %copy-start.6 = (bf16[1024,1024]{1,0:T(8,128)(2,1)S(1)}, bf16[1024,1024]{1,0:T(8,128)(2,1)}, u32[]{:S(2)}) copy-start(bf16[1024,1024]{1,0:T(8,128)(2,1)} %refs_6_.1) | copy-start | bytes 6291460
  12.3 8.0 %copy-start.9 = (f32[8]{0:T(128)S(1)}, f32[8]{0:T(128)}, u32[]{:S(2)}) copy-start(f32[8]{0:T(128)} %param.21) | copy-start | bytes 100
  12.3 8.0 %copy-start.10 = (bf16[128]{0:T(256)(128)(2,1)S(1)}, bf16[128]{0:T(256)(128)(2,1)}, u32[]{:S(2)}) copy-start(bf16[128]{0:T(256)(128)(2,1)} %param.22) | copy-start | bytes 772
  13.4 5.6 %collective-permute-start.6 = (bf16[80,128]{1,0:T(8,128)(2,1)S(1)}, bf16[80,128]{1,0:T(8,128)(2,1)S(1)}, u32[]{:S(2)}, u32[]{:S(2)}) collective-permute-start(bf16[80,128]{1,0:T(8,128)(2,1)S(1)} %shard_map.138.refs_0_), channel_id=1, source_target_pairs={{0,2},{2,4},{4,6},{6,0},{1,3},{3,5},{5,7},{7,1},{8,10},{10,12},{12... | collective-permute-start | bytes 61448 | tf_op jit(solution)/shard_map/ppermute | solution.py:40
  13.5 5.6 %collective-permute-start.5 = (bf16[80,128]{1,0:T(8,128)(2,1)S(1)}, bf16[80,128]{1,0:T(8,128)(2,1)S(1)}, u32[]{:S(2)}, u32[]{:S(2)}) collective-permute-start(bf16[80,128]{1,0:T(8,128)(2,1)S(1)} %shard_map.138.refs_0_), channel_id=1, source_target_pairs={{0,4},{2,6},{4,0},{6,2},{1,5},{3,7},{5,1},{7,3},{8,12},{10,14},{12... | collective-permute-start | bytes 61448 | tf_op jit(solution)/shard_map/ppermute | solution.py:40
  16.5 3.8 %collective-permute-start.4 = (bf16[80,128]{1,0:T(8,128)(2,1)S(1)}, bf16[80,128]{1,0:T(8,128)(2,1)S(1)}, u32[]{:S(2)}, u32[]{:S(2)}) collective-permute-start(bf16[80,128]{1,0:T(8,128)(2,1)S(1)} %shard_map.138.refs_0_), channel_id=1, source_target_pairs={{0,6},{2,0},{4,2},{6,4},{1,7},{3,1},{5,3},{7,5},{8,14},{10,8},{12,... | collective-permute-start | bytes 61448 | tf_op jit(solution)/shard_map/ppermute | solution.py:40
  20.3 14.7 %copy-start.1 = (bf16[512,4096]{1,0:T(8,128)(2,1)S(1)}, bf16[512,4096]{1,0:T(8,128)(2,1)}, u32[]{:S(2)}) copy-start(bf16[512,4096]{1,0:T(8,128)(2,1)} %w_down.1) | copy-start | bytes 12582916
  21.1 1.2 %collective-permute-start.7 = (bf16[4,512]{1,0:T(4,128)(2,1)S(1)}, bf16[4,512]{1,0:T(4,128)(2,1)S(1)}, u32[]{:S(2)}, u32[]{:S(2)}) collective-permute-start(bf16[4,512]{1,0:T(4,128)(2,1)S(1)} %get-tuple-element.14), channel_id=1, source_target_pairs={{0,1},{1,0},{2,3},{3,2},{4,5},{5,4},{6,7},{7,6},{8,9},{9,8},{10,11... | collective-permute-start | bytes 12296 | tf_op jit(solution)/shard_map/ppermute | solution.py:334
  22.2 12.8 %copy-start = (bf16[4096,512]{1,0:T(8,128)(2,1)S(1)}, bf16[4096,512]{1,0:T(8,128)(2,1)}, u32[]{:S(2)}) copy-start(bf16[4096,512]{1,0:T(8,128)(2,1)} %w_up.1) | copy-start | bytes 12582916
  22.2 12.8 %copy-start.2 = (bf16[4096]{0:T(1024)(128)(2,1)S(1)}, bf16[4096]{0:T(1024)(128)(2,1)}, u32[]{:S(2)}) copy-start(bf16[4096]{0:T(1024)(128)(2,1)} %param.24) | copy-start | bytes 24580

commit v4 on v3

--- a/solution.py
+++ b/solution.py
@@ -136,8 +136,7 @@
         out[span * r : span * (r + 1), :] = value.astype(BF)
 
 
-def merge_kernel(heads, rows, messages, lam, head_gain, w_out, mine, theirs, turn):
-    first = lax.axis_index("tp") == 0
+def merge_kernel(heads, rows, messages, lam, head_gain, w_out, attended, theirs, turn):
     span = 2 * heads
     joined = []
     for message in messages:
@@ -166,15 +165,25 @@
     wide = jnp.concatenate(
         [turn[pl.ds(h, rows, stride=heads), :] for h in range(heads)], axis=1
     )
-    branch = jnp.dot(wide.astype(BF), w_out[...], preferred_element_type=F32)
-    half = branch.shape[1] // 2
-    mine[...] = jnp.where(first, branch[:, :half], branch[:, half:]).astype(BF)
-    theirs[...] = jnp.where(first, branch[:, half:], branch[:, :half]).astype(BF)
-
-
-def hidden_kernel(tokens, mine, received, copies, hidden):
-    branch = mine[...].astype(F32) + received[...].astype(F32)
-    value = (tokens[...].astype(F32) + branch).astype(BF)
+    half = theirs.shape[1]
+    at = pl.ds(pl.multiple_of((1 - lax.axis_index("tp")) * half, LANES), half)
+    wide = wide.astype(BF)
+    theirs[...] = jnp.dot(wide, w_out[:, at], preferred_element_type=F32).astype(BF)
+    attended[...] = wide
+
+
+def branch_kernel(tokens, attended, w_out, out):
+    half = out.shape[1] // 2
+    at = pl.ds(pl.multiple_of(lax.axis_index("tp") * half, LANES), half)
+    branch = jnp.dot(attended[...], w_out[:, at], preferred_element_type=F32).astype(BF)
+    out[:, :half] = branch.astype(F32)
+    out[:, half:] = tokens[...].astype(F32)
+
+
+def hidden_kernel(base, received, copies, hidden):
+    half = hidden.shape[1]
+    branch = base[:, :half] + received[...].astype(F32)
+    value = (base[:, half:] + branch).astype(BF)
     hidden[...] = value
     for k in range(copies.shape[0]):
         copies[k] = value
@@ -323,20 +332,21 @@
     def merge(*refs):
         merge_kernel(heads, rows, refs[:count], *refs[count:])
 
-    mine, theirs = call(
+    attended, theirs = call(
         merge,
-        (shape((rows, width), BF), shape((rows, width), BF)),
+        (shape((rows, heads * VD), BF), shape((rows, width), BF)),
         (*messages, lam.reshape(1, heads), head_gain.reshape(1, VD), w_out),
         5,
         8,
         [(heads * rows, LANES)],
     )
     received = lax.ppermute(theirs, "tp", swap)
+    base = call(branch_kernel, shape((rows, 2 * width), F32), (held, attended, w_out), 5)
     devices = dp_count * kv_count * tp_count
     copies, hidden = call(
         hidden_kernel,
         (shape((devices, rows, width), BF), shape((rows, width), BF)),
-        (held, mine, received),
+        (base, received),
         2,
     )
     everyone = lax.all_to_all(copies, axes, 0, 0, tiled=True)

time: 47 us -> 46.9 us (level)
    pallas_call x6 -> x7, Pallas kernels: 4.17 us -> 4.29 us  [call(): pl.pallas_call(kernel, out_shape=shapes, in_specs=[VMEM] * len(inputs), o...]
where the time goes in v4:
time: 46.9 us; the launch traced here: 46.7 us
  blocking collectives  22.7 us (48%)
  starting transfers between devices  10.1 us (22%)
  waiting for transfers between devices  7.97 us (17%)
  Pallas kernels  5.15 us (11%)
  local copies, waits for them, and re-layouts  0.7 us (1%)
    all_to_all x1, blocking collectives, local(): everyone = lax.all_to_all(copies, axes, 0, 0, tiled=True)  12.8 us
    all_to_all x1, blocking collectives, local(): terms = lax.all_to_all(term, axes, 0, 0, tiled=True)  9.86 us
    ppermute x6, starting transfers between devices, everyones(): got.append(lax.ppermute(value, axis, list(enumerate(pairs))))  9.63 us
    ppermute x6, waiting for transfers between devices, everyones(): got.append(lax.ppermute(value, axis, list(enumerate(pairs))))  6.9 us
    pallas_call x7, Pallas kernels, call(): pl.pallas_call(kernel, out_shape=shapes, in_specs=[VMEM] * len(inputs), o...  4.29 us
  transfers between devices with their start and end apart: 8, of which 6 were waited for; matrix products, arithmetic and copies ran while one was open for 0% of the time, Pallas kernels for 2%

profile of v4, /device:TPU:0, one launch (start us, length us, event | category | flops | bytes accessed | tf_op | source)
XLA Modules:
  0.0 46.7 jit_solution(1334358522332472840)
XLA Ops:
  0.0 0.5 %collective-permute-start = (bf16[4,512]{1,0:T(4,128)(2,1)}, bf16[4,512]{1,0:T(4,128)(2,1)S(1)}, u32[]{:S(2)}, u32[]{:S(2)}) collective-permute-start(bf16[4,512]{1,0:T(4,128)(2,1)} %refs_0_.1), channel_id=1, source_target_pairs={{0,1},{1,0},{2,3},{3,2},{4,5},{5,4},{6,7},{7,6},{8,9},{9,8},{10,11... | collective-permute-start | bytes 12296 | tf_op jit(solution)/shard_map/ppermute | solution.py:301
  0.5 0.9 %shard_map.136 = (bf16[4,512]{1,0:T(4,128)(2,1)S(1)}, bf16[8,128]{1,0:T(8,128)(2,1)S(1)}) custom-call(bf16[4,512]{1,0:T(4,128)(2,1)} %refs_0_.1, bf16[8,128]{1,0:T(8,128)(2,1)} %bitcast.11), custom_call_target="tpu_custom_call" | custom-call | flops 8589934592 | bytes 8388608 | tf_op jit(solution)/shard_map/pallas_call | solution.py:239
  1.4 0.2 collective-permute-done.other
  1.5 0.6 %copy-done.3 = bf16[1024,1024]{1,0:T(8,128)(2,1)S(1)} copy-done((bf16[1024,1024]{1,0:T(8,128)(2,1)S(1)}, bf16[1024,1024]{1,0:T(8,128)(2,1)}, u32[]{:S(2)}) %copy-start.3) | copy-done | bytes 2097176
  2.1 0.0 copy-done.7
  2.1 0.1 copy-done.8
  2.2 0.4 shard_map.137.refs_0_
  2.6 3.6 %collective-permute-start.3 = (f32[4,1408]{1,0:T(4,128)S(1)}, f32[4,1408]{1,0:T(4,128)S(1)}, u32[]{:S(2)}, u32[]{:S(2)}) collective-permute-start(f32[4,1408]{1,0:T(4,128)S(1)} %shard_map.137.refs_0_), channel_id=1, source_target_pairs={{0,4},{2,0},{4,6},{6,2},{1,5},{3,1},{5,7},{7,3},{8,12},{10,8},{12,... | collective-permute-start | bytes 67592 | tf_op jit(solution)/shard_map/ppermute | solution.py:40
  6.3 1.3 %collective-permute-start.2 = (f32[4,1408]{1,0:T(4,128)S(1)}, f32[4,1408]{1,0:T(4,128)S(1)}, u32[]{:S(2)}, u32[]{:S(2)}) collective-permute-start(f32[4,1408]{1,0:T(4,128)S(1)} %shard_map.137.refs_0_), channel_id=1, source_target_pairs={{0,6},{2,4},{4,2},{6,0},{1,7},{3,5},{5,3},{7,1},{8,14},{10,12},{12... | collective-permute-start | bytes 67592 | tf_op jit(solution)/shard_map/ppermute | solution.py:40
  7.6 0.8 %collective-permute-start.1 = (f32[4,1408]{1,0:T(4,128)S(1)}, f32[4,1408]{1,0:T(4,128)S(1)}, u32[]{:S(2)}, u32[]{:S(2)}) collective-permute-start(f32[4,1408]{1,0:T(4,128)S(1)} %shard_map.137.refs_0_), channel_id=1, source_target_pairs={{0,2},{2,6},{4,0},{6,4},{1,3},{3,7},{5,1},{7,5},{8,10},{10,14},{12... | collective-permute-start | bytes 67592 | tf_op jit(solution)/shard_map/ppermute | solution.py:40
  8.4 0.0 collective-permute-done.3.refs_3_
  8.4 3.5 %collective-permute-done.2.refs_2_ = f32[4,1408]{1,0:T(4,128)S(1)} collective-permute-done((f32[4,1408]{1,0:T(4,128)S(1)}, f32[4,1408]{1,0:T(4,128)S(1)}, u32[]{:S(2)}, u32[]{:S(2)}) %collective-permute-start.2) | collective-permute-done | bytes 22560 | tf_op jit(solution)/shard_map/ppermute | solution.py:40
  11.9 0.4 collective-permute-done.1.refs_1_
  12.3 0.0 copy-start.6
  12.3 0.0 copy-start.9
  12.3 0.0 copy-start.10
  12.4 1.1 %shard_map.138.refs_0_ = bf16[80,128]{1,0:T(8,128)(2,1)S(1)} custom-call(f32[4,1408]{1,0:T(4,128)S(1)} %shard_map.137.refs_0_, f32[4,1408]{1,0:T(4,128)S(1)} %collective-permute-done.1.refs_1_, f32[4,1408]{1,0:T(4,128)S(1)} %collective-permute-done.2.refs_2_, f32[4,1408]{1,0:T(4,128)S(1)} %collective-permute-done.3.refs_3_, f32[8,128]{1,0:T(8,128)S(1)} %copy-done.11, ...), custom_call_target="tpu_custom_call" | custom-call | flops 8589934592 | bytes 8388608 | tf_op jit(solution)/shard_map/pallas_call | solution.py:262
  13.4 0.1 collective-permute-start.6
  13.5 3.0 %collective-permute-start.5 = (bf16[80,128]{1,0:T(8,128)(2,1)S(1)}, bf16[80,128]{1,0:T(8,128)(2,1)S(1)}, u32[]{:S(2)}, u32[]{:S(2)}) collective-permute-start(bf16[80,128]{1,0:T(8,128)(2,1)S(1)} %shard_map.138.refs_0_), channel_id=1, source_target_pairs={{0,4},{2,6},{4,0},{6,2},{1,5},{3,7},{5,1},{7,3},{8,12},{10,14},{12... | collective-permute-start | bytes 61448 | tf_op jit(solution)/shard_map/ppermute | solution.py:40
  16.5 0.8 %collective-permute-start.4 = (bf16[80,128]{1,0:T(8,128)(2,1)S(1)}, bf16[80,128]{1,0:T(8,128)(2,1)S(1)}, u32[]{:S(2)}, u32[]{:S(2)}) collective-permute-start(bf16[80,128]{1,0:T(8,128)(2,1)S(1)} %shard_map.138.refs_0_), channel_id=1, source_target_pairs={{0,6},{2,0},{4,2},{6,4},{1,7},{3,1},{5,3},{7,5},{8,14},{10,8},{12,... | collective-permute-start | bytes 61448 | tf_op jit(solution)/shard_map/ppermute | solution.py:40
  17.3 1.8 %collective-permute-done.6.refs_3_ = bf16[80,128]{1,0:T(8,128)(2,1)S(1)} collective-permute-done((bf16[80,128]{1,0:T(8,128)(2,1)S(1)}, bf16[80,128]{1,0:T(8,128)(2,1)S(1)}, u32[]{:S(2)}, u32[]{:S(2)}) %collective-permute-start.6) | collective-permute-done | bytes 20512 | tf_op jit(solution)/shard_map/ppermute | solution.py:40
  19.1 0.0 collective-permute-done.5.refs_2_
  19.1 1.2 %collective-permute-done.4.refs_1_ = bf16[80,128]{1,0:T(8,128)(2,1)S(1)} collective-permute-done((bf16[80,128]{1,0:T(8,128)(2,1)S(1)}, bf16[80,128]{1,0:T(8,128)(2,1)S(1)}, u32[]{:S(2)}, u32[]{:S(2)}) %collective-permute-start.4) | collective-permute-done | bytes 20512 | tf_op jit(solution)/shard_map/ppermute | solution.py:40
  20.3 0.0 copy-start.1
  20.3 0.6 %shard_map.139 = (bf16[4,1024]{1,0:T(4,128)(2,1)S(1)}, bf16[4,512]{1,0:T(4,128)(2,1)S(1)}) custom-call(bf16[80,128]{1,0:T(8,128)(2,1)S(1)} %shard_map.138.refs_0_, bf16[80,128]{1,0:T(8,128)(2,1)S(1)} %collective-permute-done.4.refs_1_, bf16[80,128]{1,0:T(8,128)(2,1)S(1)} %collective-permute-done.5.refs_2_, ...), custom_call_target="tpu_custom_call" | custom-call | flops 8589934592 | bytes 8388608 | tf_op jit(solution)/shard_map/pallas_call | solution.py:262
  20.9 0.0 collective-permute-start.7
  20.9 0.3 shard_map.140.base
  21.2 0.9 %collective-permute-done.7.received = bf16[4,512]{1,0:T(4,128)(2,1)S(1)} collective-permute-done((bf16[4,512]{1,0:T(4,128)(2,1)S(1)}, bf16[4,512]{1,0:T(4,128)(2,1)S(1)}, u32[]{:S(2)}, u32[]{:S(2)}) %collective-permute-start.7) | collective-permute-done | bytes 4128 | tf_op jit(solution)/shard_map/ppermute | solution.py:343
  22.1 12.8 %all_to_all.10.everyone = bf16[32,4,512]{2,1,0:T(4,128)(2,1)S(1)} all-to-all(bf16[32,4,512]{2,1,0:T(4,128)(2,1)S(1)} %get-tuple-element.15), channel_id=1, replica_groups=mesh['dp'=4,'kv'=4,'tp'=2] {'dp','kv','tp'}, dimensions={0} | all-to-all | bytes 262144 | tf_op jit(solution)/shard_map/all_to_all | solution.py:352
  34.9 1.3 %shard_map.142 = bf16[32,4,512]{2,1,0:T(4,128)(2,1)S(1)} custom-call(bf16[32,4,512]{2,1,0:T(4,128)(2,1)S(1)} %all_to_all.10.everyone, bf16[32,128]{1,0:T(8,128)(2,1)S(1)} %bitcast.6, bf16[4096,512]{1,0:T(8,128)(2,1)S(1)} %copy-done, bf16[512,4096]{1,0:T(8,128)(2,1)S(1)} %copy-done.1), custom_call_target="tpu_custom_call" | custom-call | flops 1073741824 | bytes 1048576 | tf_op jit(solution)/shard_map/pallas_call | solution.py:262
  36.2 9.9 %all_to_all.11.terms = bf16[32,4,512]{2,1,0:T(4,128)(2,1)S(1)} all-to-all(bf16[32,4,512]{2,1,0:T(4,128)(2,1)S(1)} %shard_map.142), channel_id=1, replica_groups=mesh['dp'=4,'kv'=4,'tp'=2] {'dp','kv','tp'}, dimensions={0} | all-to-all | bytes 262144 | tf_op jit(solution)/shard_map/all_to_all | solution.py:359
  46.1 0.6 %shard_map.143 = bf16[4,512]{1,0:T(4,128)(2,1)} custom-call(bf16[32,4,512]{2,1,0:T(4,128)(2,1)S(1)} %all_to_all.11.terms, bf16[4,512]{1,0:T(4,128)(2,1)S(1)} %get-tuple-element.16.hidden), custom_call_target="tpu_custom_call" | custom-call | flops 1073741824 | bytes 1048576 | tf_op jit(solution)/shard_map/pallas_call | solution.py:262
  (18 shorter events, 0.1 us)
Async XLA Ops:
  0.0 1.5 %collective-permute-start = (bf16[4,512]{1,0:T(4,128)(2,1)}, bf16[4,512]{1,0:T(4,128)(2,1)S(1)}, u32[]{:S(2)}, u32[]{:S(2)}) collective-permute-start(bf16[4,512]{1,0:T(4,128)(2,1)} %refs_0_.1), channel_id=1, source_target_pairs={{0,1},{1,0},{2,3},{3,2},{4,5},{5,4},{6,7},{7,6},{8,9},{9,8},{10,11... | collective-permute-start | bytes 12296 | tf_op jit(solution)/shard_map/ppermute | solution.py:301
  0.5 1.6 %copy-start.3 = (bf16[1024,1024]{1,0:T(8,128)(2,1)S(1)}, bf16[1024,1024]{1,0:T(8,128)(2,1)}, u32[]{:S(2)}) copy-start(bf16[1024,1024]{1,0:T(8,128)(2,1)} %w_query.1) | copy-start | bytes 6291460
  0.5 1.6 %copy-start.7 = (bf16[1024,128]{1,0:T(8,128)(2,1)S(1)}, bf16[1024,128]{1,0:T(8,128)(2,1)}, u32[]{:S(2)}) copy-start(bf16[1024,128]{1,0:T(8,128)(2,1)} %w_key.1) | copy-start | bytes 786436
  0.5 1.7 %copy-start.8 = (bf16[1024,128]{1,0:T(8,128)(2,1)S(1)}, bf16[1024,128]{1,0:T(8,128)(2,1)}, u32[]{:S(2)}) copy-start(bf16[1024,128]{1,0:T(8,128)(2,1)} %w_value.1) | copy-start | bytes 786436
  2.2 10.1 %copy-start.4 = (bf16[4,2048,1,128]{3,1,2,0:T(8,128)(2,1)S(1)}, bf16[4,2048,1,128]{3,1,2,0:T(8,128)(2,1)}, u32[]{:S(2)}) copy-start(bf16[4,2048,1,128]{3,1,2,0:T(8,128)(2,1)} %param.19) | copy-start | bytes 6291460
  2.2 10.1 %copy-start.5 = (bf16[4,2048,1,128]{3,1,2,0:T(8,128)(2,1)S(1)}, bf16[4,2048,1,128]{3,1,2,0:T(8,128)(2,1)}, u32[]{:S(2)}) copy-start(bf16[4,2048,1,128]{3,1,2,0:T(8,128)(2,1)} %param.20) | copy-start | bytes 6291460
  2.2 10.1 %copy-start.11 = (f32[8,128]{1,0:T(8,128)S(1)}, f32[8,128]{1,0:T(8,128)}, u32[]{:S(2)}) copy-start(f32[8,128]{1,0:T(8,128)} %constant.2.clone.refs_4_) | copy-start | bytes 12292
  2.6 5.8 %collective-permute-start.3 = (f32[4,1408]{1,0:T(4,128)S(1)}, f32[4,1408]{1,0:T(4,128)S(1)}, u32[]{:S(2)}, u32[]{:S(2)}) collective-permute-start(f32[4,1408]{1,0:T(4,128)S(1)} %shard_map.137.refs_0_), channel_id=1, source_target_pairs={{0,4},{2,0},{4,6},{6,2},{1,5},{3,1},{5,7},{7,3},{8,12},{10,8},{12,... | collective-permute-start | bytes 67592 | tf_op jit(solution)/shard_map/ppermute | solution.py:40
  6.3 5.6 %collective-permute-start.2 = (f32[4,1408]{1,0:T(4,128)S(1)}, f32[4,1408]{1,0:T(4,128)S(1)}, u32[]{:S(2)}, u32[]{:S(2)}) collective-permute-start(f32[4,1408]{1,0:T(4,128)S(1)} %shard_map.137.refs_0_), channel_id=1, source_target_pairs={{0,6},{2,4},{4,2},{6,0},{1,7},{3,5},{5,3},{7,1},{8,14},{10,12},{12... | collective-permute-start | bytes 67592 | tf_op jit(solution)/shard_map/ppermute | solution.py:40
  7.6 4.7 %collective-permute-start.1 = (f32[4,1408]{1,0:T(4,128)S(1)}, f32[4,1408]{1,0:T(4,128)S(1)}, u32[]{:S(2)}, u32[]{:S(2)}) collective-permute-start(f32[4,1408]{1,0:T(4,128)S(1)} %shard_map.137.refs_0_), channel_id=1, source_target_pairs={{0,2},{2,6},{4,0},{6,4},{1,3},{3,7},{5,1},{7,5},{8,10},{10,14},{12... | collective-permute-start | bytes 67592 | tf_op jit(solution)/shard_map/ppermute | solution.py:40
  12.3 8.0 %copy-start.6 = (bf16[1024,1024]{1,0:T(8,128)(2,1)S(1)}, bf16[1024,1024]{1,0:T(8,128)(2,1)}, u32[]{:S(2)}) copy-start(bf16[1024,1024]{1,0:T(8,128)(2,1)} %w_out.1) | copy-start | bytes 6291460
  12.3 8.0 %copy-start.9 = (f32[8]{0:T(128)S(1)}, f32[8]{0:T(128)}, u32[]{:S(2)}) copy-start(f32[8]{0:T(128)} %param.21) | copy-start | bytes 100
  12.3 8.0 %copy-start.10 = (bf16[128]{0:T(256)(128)(2,1)S(1)}, bf16[128]{0:T(256)(128)(2,1)}, u32[]{:S(2)}) copy-start(bf16[128]{0:T(256)(128)(2,1)} %param.22) | copy-start | bytes 772
  13.4 5.6 %collective-permute-start.6 = (bf16[80,128]{1,0:T(8,128)(2,1)S(1)}, bf16[80,128]{1,0:T(8,128)(2,1)S(1)}, u32[]{:S(2)}, u32[]{:S(2)}) collective-permute-start(bf16[80,128]{1,0:T(8,128)(2,1)S(1)} %shard_map.138.refs_0_), channel_id=1, source_target_pairs={{0,2},{2,4},{4,6},{6,0},{1,3},{3,5},{5,7},{7,1},{8,10},{10,12},{12... | collective-permute-start | bytes 61448 | tf_op jit(solution)/shard_map/ppermute | solution.py:40
  13.5 5.6 %collective-permute-start.5 = (bf16[80,128]{1,0:T(8,128)(2,1)S(1)}, bf16[80,128]{1,0:T(8,128)(2,1)S(1)}, u32[]{:S(2)}, u32[]{:S(2)}) collective-permute-start(bf16[80,128]{1,0:T(8,128)(2,1)S(1)} %shard_map.138.refs_0_), channel_id=1, source_target_pairs={{0,4},{2,6},{4,0},{6,2},{1,5},{3,7},{5,1},{7,3},{8,12},{10,14},{12... | collective-permute-start | bytes 61448 | tf_op jit(solution)/shard_map/ppermute | solution.py:40
  16.5 3.8 %collective-permute-start.4 = (bf16[80,128]{1,0:T(8,128)(2,1)S(1)}, bf16[80,128]{1,0:T(8,128)(2,1)S(1)}, u32[]{:S(2)}, u32[]{:S(2)}) collective-permute-start(bf16[80,128]{1,0:T(8,128)(2,1)S(1)} %shard_map.138.refs_0_), channel_id=1, source_target_pairs={{0,6},{2,0},{4,2},{6,4},{1,7},{3,1},{5,3},{7,5},{8,14},{10,8},{12,... | collective-permute-start | bytes 61448 | tf_op jit(solution)/shard_map/ppermute | solution.py:40
  20.3 14.6 %copy-start.1 = (bf16[512,4096]{1,0:T(8,128)(2,1)S(1)}, bf16[512,4096]{1,0:T(8,128)(2,1)}, u32[]{:S(2)}) copy-start(bf16[512,4096]{1,0:T(8,128)(2,1)} %w_down.1) | copy-start | bytes 12582916
  20.9 1.2 %collective-permute-start.7 = (bf16[4,512]{1,0:T(4,128)(2,1)S(1)}, bf16[4,512]{1,0:T(4,128)(2,1)S(1)}, u32[]{:S(2)}, u32[]{:S(2)}) collective-permute-start(bf16[4,512]{1,0:T(4,128)(2,1)S(1)} %get-tuple-element.14), channel_id=1, source_target_pairs={{0,1},{1,0},{2,3},{3,2},{4,5},{5,4},{6,7},{7,6},{8,9},{9,8},{10,11... | collective-permute-start | bytes 12296 | tf_op jit(solution)/shard_map/ppermute | solution.py:343
  21.2 13.7 %copy-start = (bf16[4096,512]{1,0:T(8,128)(2,1)S(1)}, bf16[4096,512]{1,0:T(8,128)(2,1)}, u32[]{:S(2)}) copy-start(bf16[4096,512]{1,0:T(8,128)(2,1)} %w_up.1) | copy-start | bytes 12582916
  21.2 13.7 %copy-start.2 = (bf16[4096]{0:T(1024)(128)(2,1)S(1)}, bf16[4096]{0:T(1024)(128)(2,1)}, u32[]{:S(2)}) copy-start(bf16[4096]{0:T(1024)(128)(2,1)} %param.24) | copy-start | bytes 24580

commit v5 on v4

--- a/solution.py
+++ b/solution.py
@@ -19,8 +19,6 @@
 F32 = jnp.float32
 BF = jnp.bfloat16
 VMEM = pl.BlockSpec(memory_space=pltpu.VMEM)
-SMEM = pl.BlockSpec(memory_space=pltpu.SMEM)
-ANY = pl.BlockSpec(memory_space=pl.ANY)
 
 
 def rounds(count, first):
@@ -193,12 +191,13 @@
     devices, rows, width = everyone.shape
     blocks = devices // dps
     per = width // LANES
+    places = [(b % 2 * (blocks // 2) + b // 2) * dps for b in range(blocks)]
     gains = gain[...].astype(F32)
     square = jnp.zeros((dps * rows, width), F32)
     upward = jnp.zeros((dps * rows, w_up.shape[1]), F32)
     for b in range(blocks):
         block = jnp.concatenate(
-            [everyone[a * blocks + b].astype(F32) for a in range(dps)], axis=0
+            [everyone[places[b] + a].astype(F32) for a in range(dps)], axis=0
         )
         square = square + block * block
         scaled = (block * flat_row(gains, b * per, per)).astype(BF)
@@ -212,7 +211,7 @@
             act, w_down[:, b * width : (b + 1) * width], preferred_element_type=F32
         ).astype(BF)
         for a in range(dps):
-            out[a * blocks + b] = down[a * rows : (a + 1) * rows, :]
+            out[places[b] + a] = down[a * rows : (a + 1) * rows, :]
 
 
 def final_kernel(terms, hidden, out):
@@ -293,7 +292,7 @@
     dp_count = lax.axis_size("dp")
     positions = key_cache.shape[1]
     heads = lam.shape[0]
-    axes = ("dp", "kv", "tp")
+    axes = ("tp", "kv", "dp")
     swap = [(0, 1), (1, 0)]
     assert tp_count == 2 and key_cache.shape[2] == 1 and 6 * rows <= LANES
     shape = jax.ShapeDtypeStruct

time: 46.9 us -> 46.7 us (level)
  no operation moved by 1% of the time
where the time goes in v5:
time: 46.7 us; the launch traced here: 46.5 us
  blocking collectives  22.5 us (48%)
  starting transfers between devices  10.1 us (22%)
  waiting for transfers between devices  7.97 us (17%)
  Pallas kernels  5.15 us (11%)
  local copies, waits for them, and re-layouts  0.7 us (1%)
    all_to_all x1, blocking collectives, local(): everyone = lax.all_to_all(copies, axes, 0, 0, tiled=True)  12.6 us
    all_to_all x1, blocking collectives, local(): terms = lax.all_to_all(term, axes, 0, 0, tiled=True)  9.88 us
    ppermute x6, starting transfers between devices, everyones(): got.append(lax.ppermute(value, axis, list(enumerate(pairs))))  9.63 us
    ppermute x6, waiting for transfers between devices, everyones(): got.append(lax.ppermute(value, axis, list(enumerate(pairs))))  6.9 us
    pallas_call x7, Pallas kernels, call(): pl.pallas_call(kernel, out_shape=shapes, in_specs=[VMEM] * len(inputs), o...  4.29 us
  transfers between devices with their start and end apart: 8, of which 6 were waited for; matrix products, arithmetic and copies ran while one was open for 0% of the time, Pallas kernels for 2%

profile of v5, /device:TPU:0, one launch (start us, length us, event | category | flops | bytes accessed | tf_op | source)
XLA Modules:
  0.0 46.5 jit_solution(13766248775946216828)
XLA Ops:
  0.0 0.5 %collective-permute-start = (bf16[4,512]{1,0:T(4,128)(2,1)}, bf16[4,512]{1,0:T(4,128)(2,1)S(1)}, u32[]{:S(2)}, u32[]{:S(2)}) collective-permute-start(bf16[4,512]{1,0:T(4,128)(2,1)} %refs_0_.1), channel_id=1, source_target_pairs={{0,1},{1,0},{2,3},{3,2},{4,5},{5,4},{6,7},{7,6},{8,9},{9,8},{10,11... | collective-permute-start | bytes 12296 | tf_op jit(solution)/shard_map/ppermute | solution.py:300
  0.5 0.9 %shard_map.136 = (bf16[4,512]{1,0:T(4,128)(2,1)S(1)}, bf16[8,128]{1,0:T(8,128)(2,1)S(1)}) custom-call(bf16[4,512]{1,0:T(4,128)(2,1)} %refs_0_.1, bf16[8,128]{1,0:T(8,128)(2,1)} %bitcast.11), custom_call_target="tpu_custom_call" | custom-call | flops 8589934592 | bytes 8388608 | tf_op jit(solution)/shard_map/pallas_call | solution.py:238
  1.4 0.2 collective-permute-done.other
  1.5 0.6 %copy-done.3 = bf16[1024,1024]{1,0:T(8,128)(2,1)S(1)} copy-done((bf16[1024,1024]{1,0:T(8,128)(2,1)S(1)}, bf16[1024,1024]{1,0:T(8,128)(2,1)}, u32[]{:S(2)}) %copy-start.3) | copy-done | bytes 2097176
  2.1 0.0 copy-done.7
  2.1 0.1 copy-done.8
  2.2 0.4 shard_map.137.refs_0_
  2.6 3.6 %collective-permute-start.3 = (f32[4,1408]{1,0:T(4,128)S(1)}, f32[4,1408]{1,0:T(4,128)S(1)}, u32[]{:S(2)}, u32[]{:S(2)}) collective-permute-start(f32[4,1408]{1,0:T(4,128)S(1)} %shard_map.137.refs_0_), channel_id=1, source_target_pairs={{0,4},{2,0},{4,6},{6,2},{1,5},{3,1},{5,7},{7,3},{8,12},{10,8},{12,... | collective-permute-start | bytes 67592 | tf_op jit(solution)/shard_map/ppermute | solution.py:38
  6.3 1.3 %collective-permute-start.2 = (f32[4,1408]{1,0:T(4,128)S(1)}, f32[4,1408]{1,0:T(4,128)S(1)}, u32[]{:S(2)}, u32[]{:S(2)}) collective-permute-start(f32[4,1408]{1,0:T(4,128)S(1)} %shard_map.137.refs_0_), channel_id=1, source_target_pairs={{0,6},{2,4},{4,2},{6,0},{1,7},{3,5},{5,3},{7,1},{8,14},{10,12},{12... | collective-permute-start | bytes 67592 | tf_op jit(solution)/shard_map/ppermute | solution.py:38
  7.6 0.8 %collective-permute-start.1 = (f32[4,1408]{1,0:T(4,128)S(1)}, f32[4,1408]{1,0:T(4,128)S(1)}, u32[]{:S(2)}, u32[]{:S(2)}) collective-permute-start(f32[4,1408]{1,0:T(4,128)S(1)} %shard_map.137.refs_0_), channel_id=1, source_target_pairs={{0,2},{2,6},{4,0},{6,4},{1,3},{3,7},{5,1},{7,5},{8,10},{10,14},{12... | collective-permute-start | bytes 67592 | tf_op jit(solution)/shard_map/ppermute | solution.py:38
  8.4 0.0 collective-permute-done.3.refs_3_
  8.4 3.5 %collective-permute-done.2.refs_2_ = f32[4,1408]{1,0:T(4,128)S(1)} collective-permute-done((f32[4,1408]{1,0:T(4,128)S(1)}, f32[4,1408]{1,0:T(4,128)S(1)}, u32[]{:S(2)}, u32[]{:S(2)}) %collective-permute-start.2) | collective-permute-done | bytes 22560 | tf_op jit(solution)/shard_map/ppermute | solution.py:38
  11.9 0.4 collective-permute-done.1.refs_1_
  12.3 0.0 copy-start.6
  12.3 0.0 copy-start.9
  12.3 0.0 copy-start.10
  12.4 1.1 %shard_map.138.refs_0_ = bf16[80,128]{1,0:T(8,128)(2,1)S(1)} custom-call(f32[4,1408]{1,0:T(4,128)S(1)} %shard_map.137.refs_0_, f32[4,1408]{1,0:T(4,128)S(1)} %collective-permute-done.1.refs_1_, f32[4,1408]{1,0:T(4,128)S(1)} %collective-permute-done.2.refs_2_, f32[4,1408]{1,0:T(4,128)S(1)} %collective-permute-done.3.refs_3_, f32[8,128]{1,0:T(8,128)S(1)} %copy-done.11, ...), custom_call_target="tpu_custom_call" | custom-call | flops 8589934592 | bytes 8388608 | tf_op jit(solution)/shard_map/pallas_call | solution.py:261
  13.4 0.1 collective-permute-start.6
  13.5 3.0 %collective-permute-start.5 = (bf16[80,128]{1,0:T(8,128)(2,1)S(1)}, bf16[80,128]{1,0:T(8,128)(2,1)S(1)}, u32[]{:S(2)}, u32[]{:S(2)}) collective-permute-start(bf16[80,128]{1,0:T(8,128)(2,1)S(1)} %shard_map.138.refs_0_), channel_id=1, source_target_pairs={{0,4},{2,6},{4,0},{6,2},{1,5},{3,7},{5,1},{7,3},{8,12},{10,14},{12... | collective-permute-start | bytes 61448 | tf_op jit(solution)/shard_map/ppermute | solution.py:38
  16.5 0.8 %collective-permute-start.4 = (bf16[80,128]{1,0:T(8,128)(2,1)S(1)}, bf16[80,128]{1,0:T(8,128)(2,1)S(1)}, u32[]{:S(2)}, u32[]{:S(2)}) collective-permute-start(bf16[80,128]{1,0:T(8,128)(2,1)S(1)} %shard_map.138.refs_0_), channel_id=1, source_target_pairs={{0,6},{2,0},{4,2},{6,4},{1,7},{3,1},{5,3},{7,5},{8,14},{10,8},{12,... | collective-permute-start | bytes 61448 | tf_op jit(solution)/shard_map/ppermute | solution.py:38
  17.3 1.8 %collective-permute-done.6.refs_3_ = bf16[80,128]{1,0:T(8,128)(2,1)S(1)} collective-permute-done((bf16[80,128]{1,0:T(8,128)(2,1)S(1)}, bf16[80,128]{1,0:T(8,128)(2,1)S(1)}, u32[]{:S(2)}, u32[]{:S(2)}) %collective-permute-start.6) | collective-permute-done | bytes 20512 | tf_op jit(solution)/shard_map/ppermute | solution.py:38
  19.1 0.0 collective-permute-done.5.refs_2_
  19.1 1.2 %collective-permute-done.4.refs_1_ = bf16[80,128]{1,0:T(8,128)(2,1)S(1)} collective-permute-done((bf16[80,128]{1,0:T(8,128)(2,1)S(1)}, bf16[80,128]{1,0:T(8,128)(2,1)S(1)}, u32[]{:S(2)}, u32[]{:S(2)}) %collective-permute-start.4) | collective-permute-done | bytes 20512 | tf_op jit(solution)/shard_map/ppermute | solution.py:38
  20.3 0.0 copy-start.1
  20.3 0.6 %shard_map.139 = (bf16[4,1024]{1,0:T(4,128)(2,1)S(1)}, bf16[4,512]{1,0:T(4,128)(2,1)S(1)}) custom-call(bf16[80,128]{1,0:T(8,128)(2,1)S(1)} %shard_map.138.refs_0_, bf16[80,128]{1,0:T(8,128)(2,1)S(1)} %collective-permute-done.4.refs_1_, bf16[80,128]{1,0:T(8,128)(2,1)S(1)} %collective-permute-done.5.refs_2_, ...), custom_call_target="tpu_custom_call" | custom-call | flops 8589934592 | bytes 8388608 | tf_op jit(solution)/shard_map/pallas_call | solution.py:261
  20.9 0.0 collective-permute-start.7
  20.9 0.3 shard_map.140.base
  21.2 0.9 %collective-permute-done.7.received = bf16[4,512]{1,0:T(4,128)(2,1)S(1)} collective-permute-done((bf16[4,512]{1,0:T(4,128)(2,1)S(1)}, bf16[4,512]{1,0:T(4,128)(2,1)S(1)}, u32[]{:S(2)}, u32[]{:S(2)}) %collective-permute-start.7) | collective-permute-done | bytes 4128 | tf_op jit(solution)/shard_map/ppermute | solution.py:342
  22.1 12.6 %all_to_all.10.everyone = bf16[32,4,512]{2,1,0:T(4,128)(2,1)S(1)} all-to-all(bf16[32,4,512]{2,1,0:T(4,128)(2,1)S(1)} %get-tuple-element.15), channel_id=1, replica_groups=mesh['dp'=4,'kv'=4,'tp'=2] {'tp','kv','dp'}, dimensions={0} | all-to-all | bytes 262144 | tf_op jit(solution)/shard_map/all_to_all | solution.py:351
  34.7 1.3 %shard_map.142 = bf16[32,4,512]{2,1,0:T(4,128)(2,1)S(1)} custom-call(bf16[32,4,512]{2,1,0:T(4,128)(2,1)S(1)} %all_to_all.10.everyone, bf16[32,128]{1,0:T(8,128)(2,1)S(1)} %bitcast.6, bf16[4096,512]{1,0:T(8,128)(2,1)S(1)} %copy-done, bf16[512,4096]{1,0:T(8,128)(2,1)S(1)} %copy-done.1), custom_call_target="tpu_custom_call" | custom-call | flops 1073741824 | bytes 1048576 | tf_op jit(solution)/shard_map/pallas_call | solution.py:261
  36.0 9.9 %all_to_all.11.terms = bf16[32,4,512]{2,1,0:T(4,128)(2,1)S(1)} all-to-all(bf16[32,4,512]{2,1,0:T(4,128)(2,1)S(1)} %shard_map.142), channel_id=1, replica_groups=mesh['dp'=4,'kv'=4,'tp'=2] {'tp','kv','dp'}, dimensions={0} | all-to-all | bytes 262144 | tf_op jit(solution)/shard_map/all_to_all | solution.py:358
  45.9 0.6 %shard_map.143 = bf16[4,512]{1,0:T(4,128)(2,1)} custom-call(bf16[32,4,512]{2,1,0:T(4,128)(2,1)S(1)} %all_to_all.11.terms, bf16[4,512]{1,0:T(4,128)(2,1)S(1)} %get-tuple-element.16.hidden), custom_call_target="tpu_custom_call" | custom-call | flops 1073741824 | bytes 1048576 | tf_op jit(solution)/shard_map/pallas_call | solution.py:261
  (18 shorter events, 0.1 us)
Async XLA Ops:
  0.0 1.5 %collective-permute-start = (bf16[4,512]{1,0:T(4,128)(2,1)}, bf16[4,512]{1,0:T(4,128)(2,1)S(1)}, u32[]{:S(2)}, u32[]{:S(2)}) collective-permute-start(bf16[4,512]{1,0:T(4,128)(2,1)} %refs_0_.1), channel_id=1, source_target_pairs={{0,1},{1,0},{2,3},{3,2},{4,5},{5,4},{6,7},{7,6},{8,9},{9,8},{10,11... | collective-permute-start | bytes 12296 | tf_op jit(solution)/shard_map/ppermute | solution.py:300
  0.5 1.6 %copy-start.3 = (bf16[1024,1024]{1,0:T(8,128)(2,1)S(1)}, bf16[1024,1024]{1,0:T(8,128)(2,1)}, u32[]{:S(2)}) copy-start(bf16[1024,1024]{1,0:T(8,128)(2,1)} %w_query.1) | copy-start | bytes 6291460
  0.5 1.6 %copy-start.7 = (bf16[1024,128]{1,0:T(8,128)(2,1)S(1)}, bf16[1024,128]{1,0:T(8,128)(2,1)}, u32[]{:S(2)}) copy-start(bf16[1024,128]{1,0:T(8,128)(2,1)} %w_key.1) | copy-start | bytes 786436
  0.5 1.7 %copy-start.8 = (bf16[1024,128]{1,0:T(8,128)(2,1)S(1)}, bf16[1024,128]{1,0:T(8,128)(2,1)}, u32[]{:S(2)}) copy-start(bf16[1024,128]{1,0:T(8,128)(2,1)} %w_value.1) | copy-start | bytes 786436
  2.2 10.1 %copy-start.4 = (bf16[4,2048,1,128]{3,1,2,0:T(8,128)(2,1)S(1)}, bf16[4,2048,1,128]{3,1,2,0:T(8,128)(2,1)}, u32[]{:S(2)}) copy-start(bf16[4,2048,1,128]{3,1,2,0:T(8,128)(2,1)} %param.19) | copy-start | bytes 6291460
  2.2 10.1 %copy-start.5 = (bf16[4,2048,1,128]{3,1,2,0:T(8,128)(2,1)S(1)}, bf16[4,2048,1,128]{3,1,2,0:T(8,128)(2,1)}, u32[]{:S(2)}) copy-start(bf16[4,2048,1,128]{3,1,2,0:T(8,128)(2,1)} %param.20) | copy-start | bytes 6291460
  2.2 10.1 %copy-start.11 = (f32[8,128]{1,0:T(8,128)S(1)}, f32[8,128]{1,0:T(8,128)}, u32[]{:S(2)}) copy-start(f32[8,128]{1,0:T(8,128)} %constant.2.clone.refs_4_) | copy-start | bytes 12292
  2.6 5.8 %collective-permute-start.3 = (f32[4,1408]{1,0:T(4,128)S(1)}, f32[4,1408]{1,0:T(4,128)S(1)}, u32[]{:S(2)}, u32[]{:S(2)}) collective-permute-start(f32[4,1408]{1,0:T(4,128)S(1)} %shard_map.137.refs_0_), channel_id=1, source_target_pairs={{0,4},{2,0},{4,6},{6,2},{1,5},{3,1},{5,7},{7,3},{8,12},{10,8},{12,... | collective-permute-start | bytes 67592 | tf_op jit(solution)/shard_map/ppermute | solution.py:38
  6.3 5.6 %collective-permute-start.2 = (f32[4,1408]{1,0:T(4,128)S(1)}, f32[4,1408]{1,0:T(4,128)S(1)}, u32[]{:S(2)}, u32[]{:S(2)}) collective-permute-start(f32[4,1408]{1,0:T(4,128)S(1)} %shard_map.137.refs_0_), channel_id=1, source_target_pairs={{0,6},{2,4},{4,2},{6,0},{1,7},{3,5},{5,3},{7,1},{8,14},{10,12},{12... | collective-permute-start | bytes 67592 | tf_op jit(solution)/shard_map/ppermute | solution.py:38
  7.6 4.7 %collective-permute-start.1 = (f32[4,1408]{1,0:T(4,128)S(1)}, f32[4,1408]{1,0:T(4,128)S(1)}, u32[]{:S(2)}, u32[]{:S(2)}) collective-permute-start(f32[4,1408]{1,0:T(4,128)S(1)} %shard_map.137.refs_0_), channel_id=1, source_target_pairs={{0,2},{2,6},{4,0},{6,4},{1,3},{3,7},{5,1},{7,5},{8,10},{10,14},{12... | collective-permute-start | bytes 67592 | tf_op jit(solution)/shard_map/ppermute | solution.py:38
  12.3 8.0 %copy-start.6 = (bf16[1024,1024]{1,0:T(8,128)(2,1)S(1)}, bf16[1024,1024]{1,0:T(8,128)(2,1)}, u32[]{:S(2)}) copy-start(bf16[1024,1024]{1,0:T(8,128)(2,1)} %w_out.1) | copy-start | bytes 6291460
  12.3 8.0 %copy-start.9 = (f32[8]{0:T(128)S(1)}, f32[8]{0:T(128)}, u32[]{:S(2)}) copy-start(f32[8]{0:T(128)} %param.21) | copy-start | bytes 100
  12.3 8.0 %copy-start.10 = (bf16[128]{0:T(256)(128)(2,1)S(1)}, bf16[128]{0:T(256)(128)(2,1)}, u32[]{:S(2)}) copy-start(bf16[128]{0:T(256)(128)(2,1)} %param.22) | copy-start | bytes 772
  13.4 5.6 %collective-permute-start.6 = (bf16[80,128]{1,0:T(8,128)(2,1)S(1)}, bf16[80,128]{1,0:T(8,128)(2,1)S(1)}, u32[]{:S(2)}, u32[]{:S(2)}) collective-permute-start(bf16[80,128]{1,0:T(8,128)(2,1)S(1)} %shard_map.138.refs_0_), channel_id=1, source_target_pairs={{0,2},{2,4},{4,6},{6,0},{1,3},{3,5},{5,7},{7,1},{8,10},{10,12},{12... | collective-permute-start | bytes 61448 | tf_op jit(solution)/shard_map/ppermute | solution.py:38
  13.5 5.6 %collective-permute-start.5 = (bf16[80,128]{1,0:T(8,128)(2,1)S(1)}, bf16[80,128]{1,0:T(8,128)(2,1)S(1)}, u32[]{:S(2)}, u32[]{:S(2)}) collective-permute-start(bf16[80,128]{1,0:T(8,128)(2,1)S(1)} %shard_map.138.refs_0_), channel_id=1, source_target_pairs={{0,4},{2,6},{4,0},{6,2},{1,5},{3,7},{5,1},{7,3},{8,12},{10,14},{12... | collective-permute-start | bytes 61448 | tf_op jit(solution)/shard_map/ppermute | solution.py:38
  16.5 3.8 %collective-permute-start.4 = (bf16[80,128]{1,0:T(8,128)(2,1)S(1)}, bf16[80,128]{1,0:T(8,128)(2,1)S(1)}, u32[]{:S(2)}, u32[]{:S(2)}) collective-permute-start(bf16[80,128]{1,0:T(8,128)(2,1)S(1)} %shard_map.138.refs_0_), channel_id=1, source_target_pairs={{0,6},{2,0},{4,2},{6,4},{1,7},{3,1},{5,3},{7,5},{8,14},{10,8},{12,... | collective-permute-start | bytes 61448 | tf_op jit(solution)/shard_map/ppermute | solution.py:38
  20.3 14.4 %copy-start.1 = (bf16[512,4096]{1,0:T(8,128)(2,1)S(1)}, bf16[512,4096]{1,0:T(8,128)(2,1)}, u32[]{:S(2)}) copy-start(bf16[512,4096]{1,0:T(8,128)(2,1)} %w_down.1) | copy-start | bytes 12582916
  20.9 1.2 %collective-permute-start.7 = (bf16[4,512]{1,0:T(4,128)(2,1)S(1)}, bf16[4,512]{1,0:T(4,128)(2,1)S(1)}, u32[]{:S(2)}, u32[]{:S(2)}) collective-permute-start(bf16[4,512]{1,0:T(4,128)(2,1)S(1)} %get-tuple-element.14), channel_id=1, source_target_pairs={{0,1},{1,0},{2,3},{3,2},{4,5},{5,4},{6,7},{7,6},{8,9},{9,8},{10,11... | collective-permute-start | bytes 12296 | tf_op jit(solution)/shard_map/ppermute | solution.py:342
  21.2 13.6 %copy-start = (bf16[4096,512]{1,0:T(8,128)(2,1)S(1)}, bf16[4096,512]{1,0:T(8,128)(2,1)}, u32[]{:S(2)}) copy-start(bf16[4096,512]{1,0:T(8,128)(2,1)} %w_up.1) | copy-start | bytes 12582916
  21.2 13.6 %copy-start.2 = (bf16[4096]{0:T(1024)(128)(2,1)S(1)}, bf16[4096]{0:T(1024)(128)(2,1)}, u32[]{:S(2)}) copy-start(bf16[4096]{0:T(1024)(128)(2,1)} %param.24) | copy-start | bytes 24580

commit v6 on v3

--- a/solution.py
+++ b/solution.py
@@ -19,8 +19,6 @@
 F32 = jnp.float32
 BF = jnp.bfloat16
 VMEM = pl.BlockSpec(memory_space=pltpu.VMEM)
-SMEM = pl.BlockSpec(memory_space=pltpu.SMEM)
-ANY = pl.BlockSpec(memory_space=pl.ANY)
 
 
 def rounds(count, first):
@@ -184,12 +182,13 @@
     devices, rows, width = everyone.shape
     blocks = devices // dps
     per = width // LANES
+    places = [(b % 2 * (blocks // 2) + b // 2) * dps for b in range(blocks)]
     gains = gain[...].astype(F32)
     square = jnp.zeros((dps * rows, width), F32)
     upward = jnp.zeros((dps * rows, w_up.shape[1]), F32)
     for b in range(blocks):
         block = jnp.concatenate(
-            [everyone[a * blocks + b].astype(F32) for a in range(dps)], axis=0
+            [everyone[places[b] + a].astype(F32) for a in range(dps)], axis=0
         )
         square = square + block * block
         scaled = (block * flat_row(gains, b * per, per)).astype(BF)
@@ -203,7 +202,7 @@
             act, w_down[:, b * width : (b + 1) * width], preferred_element_type=F32
         ).astype(BF)
         for a in range(dps):
-            out[a * blocks + b] = down[a * rows : (a + 1) * rows, :]
+            out[places[b] + a] = down[a * rows : (a + 1) * rows, :]
 
 
 def final_kernel(terms, hidden, out):
@@ -284,7 +283,7 @@
     dp_count = lax.axis_size("dp")
     positions = key_cache.shape[1]
     heads = lam.shape[0]
-    axes = ("dp", "kv", "tp")
+    axes = ("tp", "kv", "dp")
     swap = [(0, 1), (1, 0)]
     assert tp_count == 2 and key_cache.shape[2] == 1 and 6 * rows <= LANES
     shape = jax.ShapeDtypeStruct

time: 47 us -> 46.9 us (level)
  no operation moved by 1% of the time
where the time goes in v6:
time: 46.9 us; the launch traced here: 46.7 us
  blocking collectives  22.5 us (48%)
  starting transfers between devices  10.1 us (22%)
  waiting for transfers between devices  8.23 us (18%)
  Pallas kernels  5.03 us (11%)
  local copies, waits for them, and re-layouts  0.7 us (1%)
    all_to_all x1, blocking collectives, local(): everyone = lax.all_to_all(copies, axes, 0, 0, tiled=True)  12.6 us
    all_to_all x1, blocking collectives, local(): terms = lax.all_to_all(term, axes, 0, 0, tiled=True)  9.88 us
    ppermute x6, starting transfers between devices, everyones(): got.append(lax.ppermute(value, axis, list(enumerate(pairs))))  9.63 us
    ppermute x6, waiting for transfers between devices, everyones(): got.append(lax.ppermute(value, axis, list(enumerate(pairs))))  6.9 us
    pallas_call x6, Pallas kernels, call(): pl.pallas_call(kernel, out_shape=shapes, in_specs=[VMEM] * len(inputs), o...  4.17 us
    ppermute x1, waiting for transfers between devices, local(): received = lax.ppermute(theirs, 'tp', swap)  1.17 us
  transfers between devices with their start and end apart: 8, of which 6 were waited for; matrix products, arithmetic and copies ran while one was open for 0% of the time, Pallas kernels for 2%

profile of v6, /device:TPU:0, one launch (start us, length us, event | category | flops | bytes accessed | tf_op | source)
XLA Modules:
  0.0 46.7 jit_solution(9361680795565182753)
XLA Ops:
  0.0 0.5 %collective-permute-start = (bf16[4,512]{1,0:T(4,128)(2,1)}, bf16[4,512]{1,0:T(4,128)(2,1)S(1)}, u32[]{:S(2)}, u32[]{:S(2)}) collective-permute-start(bf16[4,512]{1,0:T(4,128)(2,1)} %refs_0_.1), channel_id=1, source_target_pairs={{0,1},{1,0},{2,3},{3,2},{4,5},{5,4},{6,7},{7,6},{8,9},{9,8},{10,11... | collective-permute-start | bytes 12296 | tf_op jit(solution)/shard_map/ppermute | solution.py:291
  0.5 0.9 %shard_map.136 = (bf16[4,512]{1,0:T(4,128)(2,1)S(1)}, bf16[8,128]{1,0:T(8,128)(2,1)S(1)}) custom-call(bf16[4,512]{1,0:T(4,128)(2,1)} %refs_0_.1, bf16[8,128]{1,0:T(8,128)(2,1)} %bitcast.11), custom_call_target="tpu_custom_call" | custom-call | flops 8589934592 | bytes 8388608 | tf_op jit(solution)/shard_map/pallas_call | solution.py:229
  1.4 0.2 collective-permute-done.other
  1.5 0.6 %copy-done.3 = bf16[1024,1024]{1,0:T(8,128)(2,1)S(1)} copy-done((bf16[1024,1024]{1,0:T(8,128)(2,1)S(1)}, bf16[1024,1024]{1,0:T(8,128)(2,1)}, u32[]{:S(2)}) %copy-start.3) | copy-done | bytes 2097176
  2.1 0.0 copy-done.7
  2.1 0.1 copy-done.8
  2.2 0.4 shard_map.137.refs_0_
  2.6 3.6 %collective-permute-start.3 = (f32[4,1408]{1,0:T(4,128)S(1)}, f32[4,1408]{1,0:T(4,128)S(1)}, u32[]{:S(2)}, u32[]{:S(2)}) collective-permute-start(f32[4,1408]{1,0:T(4,128)S(1)} %shard_map.137.refs_0_), channel_id=1, source_target_pairs={{0,4},{2,0},{4,6},{6,2},{1,5},{3,1},{5,7},{7,3},{8,12},{10,8},{12,... | collective-permute-start | bytes 67592 | tf_op jit(solution)/shard_map/ppermute | solution.py:38
  6.3 1.3 %collective-permute-start.2 = (f32[4,1408]{1,0:T(4,128)S(1)}, f32[4,1408]{1,0:T(4,128)S(1)}, u32[]{:S(2)}, u32[]{:S(2)}) collective-permute-start(f32[4,1408]{1,0:T(4,128)S(1)} %shard_map.137.refs_0_), channel_id=1, source_target_pairs={{0,6},{2,4},{4,2},{6,0},{1,7},{3,5},{5,3},{7,1},{8,14},{10,12},{12... | collective-permute-start | bytes 67592 | tf_op jit(solution)/shard_map/ppermute | solution.py:38
  7.6 0.8 %collective-permute-start.1 = (f32[4,1408]{1,0:T(4,128)S(1)}, f32[4,1408]{1,0:T(4,128)S(1)}, u32[]{:S(2)}, u32[]{:S(2)}) collective-permute-start(f32[4,1408]{1,0:T(4,128)S(1)} %shard_map.137.refs_0_), channel_id=1, source_target_pairs={{0,2},{2,6},{4,0},{6,4},{1,3},{3,7},{5,1},{7,5},{8,10},{10,14},{12... | collective-permute-start | bytes 67592 | tf_op jit(solution)/shard_map/ppermute | solution.py:38
  8.4 0.0 collective-permute-done.3.refs_3_
  8.4 3.5 %collective-permute-done.2.refs_2_ = f32[4,1408]{1,0:T(4,128)S(1)} collective-permute-done((f32[4,1408]{1,0:T(4,128)S(1)}, f32[4,1408]{1,0:T(4,128)S(1)}, u32[]{:S(2)}, u32[]{:S(2)}) %collective-permute-start.2) | collective-permute-done | bytes 22560 | tf_op jit(solution)/shard_map/ppermute | solution.py:38
  11.9 0.4 collective-permute-done.1.refs_1_
  12.3 0.0 copy-done.4
  12.3 0.0 copy-start.6
  12.3 0.0 copy-start.9
  12.3 0.0 copy-start.10
  12.4 1.1 %shard_map.138.refs_0_ = bf16[80,128]{1,0:T(8,128)(2,1)S(1)} custom-call(f32[4,1408]{1,0:T(4,128)S(1)} %shard_map.137.refs_0_, f32[4,1408]{1,0:T(4,128)S(1)} %collective-permute-done.1.refs_1_, f32[4,1408]{1,0:T(4,128)S(1)} %collective-permute-done.2.refs_2_, f32[4,1408]{1,0:T(4,128)S(1)} %collective-permute-done.3.refs_3_, f32[8,128]{1,0:T(8,128)S(1)} %copy-done.11, ...), custom_call_target="tpu_custom_call" | custom-call | flops 8589934592 | bytes 8388608 | tf_op jit(solution)/shard_map/pallas_call | solution.py:252
  13.4 0.1 collective-permute-start.6
  13.5 3.0 %collective-permute-start.5 = (bf16[80,128]{1,0:T(8,128)(2,1)S(1)}, bf16[80,128]{1,0:T(8,128)(2,1)S(1)}, u32[]{:S(2)}, u32[]{:S(2)}) collective-permute-start(bf16[80,128]{1,0:T(8,128)(2,1)S(1)} %shard_map.138.refs_0_), channel_id=1, source_target_pairs={{0,4},{2,6},{4,0},{6,2},{1,5},{3,7},{5,1},{7,3},{8,12},{10,14},{12... | collective-permute-start | bytes 61448 | tf_op jit(solution)/shard_map/ppermute | solution.py:38
  16.5 0.8 %collective-permute-start.4 = (bf16[80,128]{1,0:T(8,128)(2,1)S(1)}, bf16[80,128]{1,0:T(8,128)(2,1)S(1)}, u32[]{:S(2)}, u32[]{:S(2)}) collective-permute-start(bf16[80,128]{1,0:T(8,128)(2,1)S(1)} %shard_map.138.refs_0_), channel_id=1, source_target_pairs={{0,6},{2,0},{4,2},{6,4},{1,7},{3,1},{5,3},{7,5},{8,14},{10,8},{12,... | collective-permute-start | bytes 61448 | tf_op jit(solution)/shard_map/ppermute | solution.py:38
  17.3 1.8 %collective-permute-done.6.refs_3_ = bf16[80,128]{1,0:T(8,128)(2,1)S(1)} collective-permute-done((bf16[80,128]{1,0:T(8,128)(2,1)S(1)}, bf16[80,128]{1,0:T(8,128)(2,1)S(1)}, u32[]{:S(2)}, u32[]{:S(2)}) %collective-permute-start.6) | collective-permute-done | bytes 20512 | tf_op jit(solution)/shard_map/ppermute | solution.py:38
  19.1 0.0 collective-permute-done.5.refs_2_
  19.1 1.2 %collective-permute-done.4.refs_1_ = bf16[80,128]{1,0:T(8,128)(2,1)S(1)} collective-permute-done((bf16[80,128]{1,0:T(8,128)(2,1)S(1)}, bf16[80,128]{1,0:T(8,128)(2,1)S(1)}, u32[]{:S(2)}, u32[]{:S(2)}) %collective-permute-start.4) | collective-permute-done | bytes 20512 | tf_op jit(solution)/shard_map/ppermute | solution.py:38
  20.3 0.0 copy-start.1
  20.3 0.7 %shard_map.139 = (bf16[4,512]{1,0:T(4,128)(2,1)S(1)}, bf16[4,512]{1,0:T(4,128)(2,1)S(1)}) custom-call(bf16[80,128]{1,0:T(8,128)(2,1)S(1)} %shard_map.138.refs_0_, bf16[80,128]{1,0:T(8,128)(2,1)S(1)} %collective-permute-done.4.refs_1_, bf16[80,128]{1,0:T(8,128)(2,1)S(1)} %collective-permute-done.5.refs_2_, ...), custom_call_target="tpu_custom_call" | custom-call | flops 8589934592 | bytes 8388608 | tf_op jit(solution)/shard_map/pallas_call | solution.py:252
  21.1 0.0 collective-permute-start.7
  21.1 1.2 %collective-permute-done.7.received = bf16[4,512]{1,0:T(4,128)(2,1)S(1)} collective-permute-done((bf16[4,512]{1,0:T(4,128)(2,1)S(1)}, bf16[4,512]{1,0:T(4,128)(2,1)S(1)}, u32[]{:S(2)}, u32[]{:S(2)}) %collective-permute-start.7) | collective-permute-done | bytes 4128 | tf_op jit(solution)/shard_map/ppermute | solution.py:333
  22.3 12.6 %all_to_all.10.everyone = bf16[32,4,512]{2,1,0:T(4,128)(2,1)S(1)} all-to-all(bf16[32,4,512]{2,1,0:T(4,128)(2,1)S(1)} %get-tuple-element.15), channel_id=1, replica_groups=mesh['dp'=4,'kv'=4,'tp'=2] {'tp','kv','dp'}, dimensions={0} | all-to-all | bytes 262144 | tf_op jit(solution)/shard_map/all_to_all | solution.py:341
  34.9 1.3 %shard_map.141 = bf16[32,4,512]{2,1,0:T(4,128)(2,1)S(1)} custom-call(bf16[32,4,512]{2,1,0:T(4,128)(2,1)S(1)} %all_to_all.10.everyone, bf16[32,128]{1,0:T(8,128)(2,1)S(1)} %bitcast.6, bf16[4096,512]{1,0:T(8,128)(2,1)S(1)} %copy-done, bf16[512,4096]{1,0:T(8,128)(2,1)S(1)} %copy-done.1), custom_call_target="tpu_custom_call" | custom-call | flops 1073741824 | bytes 1048576 | tf_op jit(solution)/shard_map/pallas_call | solution.py:252
  36.2 9.9 %all_to_all.11.terms = bf16[32,4,512]{2,1,0:T(4,128)(2,1)S(1)} all-to-all(bf16[32,4,512]{2,1,0:T(4,128)(2,1)S(1)} %shard_map.141), channel_id=1, replica_groups=mesh['dp'=4,'kv'=4,'tp'=2] {'tp','kv','dp'}, dimensions={0} | all-to-all | bytes 262144 | tf_op jit(solution)/shard_map/all_to_all | solution.py:348
  46.0 0.6 %shard_map.142 = bf16[4,512]{1,0:T(4,128)(2,1)} custom-call(bf16[32,4,512]{2,1,0:T(4,128)(2,1)S(1)} %all_to_all.11.terms, bf16[4,512]{1,0:T(4,128)(2,1)S(1)} %get-tuple-element.16.hidden), custom_call_target="tpu_custom_call" | custom-call | flops 1073741824 | bytes 1048576 | tf_op jit(solution)/shard_map/pallas_call | solution.py:252
  (17 shorter events, 0.0 us)
Async XLA Ops:
  0.0 1.5 %collective-permute-start = (bf16[4,512]{1,0:T(4,128)(2,1)}, bf16[4,512]{1,0:T(4,128)(2,1)S(1)}, u32[]{:S(2)}, u32[]{:S(2)}) collective-permute-start(bf16[4,512]{1,0:T(4,128)(2,1)} %refs_0_.1), channel_id=1, source_target_pairs={{0,1},{1,0},{2,3},{3,2},{4,5},{5,4},{6,7},{7,6},{8,9},{9,8},{10,11... | collective-permute-start | bytes 12296 | tf_op jit(solution)/shard_map/ppermute | solution.py:291
  0.5 1.6 %copy-start.3 = (bf16[1024,1024]{1,0:T(8,128)(2,1)S(1)}, bf16[1024,1024]{1,0:T(8,128)(2,1)}, u32[]{:S(2)}) copy-start(bf16[1024,1024]{1,0:T(8,128)(2,1)} %w_query.1) | copy-start | bytes 6291460
  0.5 1.6 %copy-start.7 = (bf16[1024,128]{1,0:T(8,128)(2,1)S(1)}, bf16[1024,128]{1,0:T(8,128)(2,1)}, u32[]{:S(2)}) copy-start(bf16[1024,128]{1,0:T(8,128)(2,1)} %w_key.1) | copy-start | bytes 786436
  0.5 1.7 %copy-start.8 = (bf16[1024,128]{1,0:T(8,128)(2,1)S(1)}, bf16[1024,128]{1,0:T(8,128)(2,1)}, u32[]{:S(2)}) copy-start(bf16[1024,128]{1,0:T(8,128)(2,1)} %w_value.1) | copy-start | bytes 786436
  2.2 10.1 %copy-start.4 = (bf16[4,2048,1,128]{3,1,2,0:T(8,128)(2,1)S(1)}, bf16[4,2048,1,128]{3,1,2,0:T(8,128)(2,1)}, u32[]{:S(2)}) copy-start(bf16[4,2048,1,128]{3,1,2,0:T(8,128)(2,1)} %param.19) | copy-start | bytes 6291460
  2.2 10.1 %copy-start.5 = (bf16[4,2048,1,128]{3,1,2,0:T(8,128)(2,1)S(1)}, bf16[4,2048,1,128]{3,1,2,0:T(8,128)(2,1)}, u32[]{:S(2)}) copy-start(bf16[4,2048,1,128]{3,1,2,0:T(8,128)(2,1)} %param.20) | copy-start | bytes 6291460
  2.2 10.1 %copy-start.11 = (f32[8,128]{1,0:T(8,128)S(1)}, f32[8,128]{1,0:T(8,128)}, u32[]{:S(2)}) copy-start(f32[8,128]{1,0:T(8,128)} %constant.2.clone.refs_4_) | copy-start | bytes 12292
  2.6 5.8 %collective-permute-start.3 = (f32[4,1408]{1,0:T(4,128)S(1)}, f32[4,1408]{1,0:T(4,128)S(1)}, u32[]{:S(2)}, u32[]{:S(2)}) collective-permute-start(f32[4,1408]{1,0:T(4,128)S(1)} %shard_map.137.refs_0_), channel_id=1, source_target_pairs={{0,4},{2,0},{4,6},{6,2},{1,5},{3,1},{5,7},{7,3},{8,12},{10,8},{12,... | collective-permute-start | bytes 67592 | tf_op jit(solution)/shard_map/ppermute | solution.py:38
  6.3 5.6 %collective-permute-start.2 = (f32[4,1408]{1,0:T(4,128)S(1)}, f32[4,1408]{1,0:T(4,128)S(1)}, u32[]{:S(2)}, u32[]{:S(2)}) collective-permute-start(f32[4,1408]{1,0:T(4,128)S(1)} %shard_map.137.refs_0_), channel_id=1, source_target_pairs={{0,6},{2,4},{4,2},{6,0},{1,7},{3,5},{5,3},{7,1},{8,14},{10,12},{12... | collective-permute-start | bytes 67592 | tf_op jit(solution)/shard_map/ppermute | solution.py:38
  7.6 4.7 %collective-permute-start.1 = (f32[4,1408]{1,0:T(4,128)S(1)}, f32[4,1408]{1,0:T(4,128)S(1)}, u32[]{:S(2)}, u32[]{:S(2)}) collective-permute-start(f32[4,1408]{1,0:T(4,128)S(1)} %shard_map.137.refs_0_), channel_id=1, source_target_pairs={{0,2},{2,6},{4,0},{6,4},{1,3},{3,7},{5,1},{7,5},{8,10},{10,14},{12... | collective-permute-start | bytes 67592 | tf_op jit(solution)/shard_map/ppermute | solution.py:38
  12.3 8.0 %copy-start.6 = (bf16[1024,1024]{1,0:T(8,128)(2,1)S(1)}, bf16[1024,1024]{1,0:T(8,128)(2,1)}, u32[]{:S(2)}) copy-start(bf16[1024,1024]{1,0:T(8,128)(2,1)} %refs_6_.1) | copy-start | bytes 6291460
  12.3 8.0 %copy-start.9 = (f32[8]{0:T(128)S(1)}, f32[8]{0:T(128)}, u32[]{:S(2)}) copy-start(f32[8]{0:T(128)} %param.21) | copy-start | bytes 100
  12.3 8.0 %copy-start.10 = (bf16[128]{0:T(256)(128)(2,1)S(1)}, bf16[128]{0:T(256)(128)(2,1)}, u32[]{:S(2)}) copy-start(bf16[128]{0:T(256)(128)(2,1)} %param.22) | copy-start | bytes 772
  13.4 5.6 %collective-permute-start.6 = (bf16[80,128]{1,0:T(8,128)(2,1)S(1)}, bf16[80,128]{1,0:T(8,128)(2,1)S(1)}, u32[]{:S(2)}, u32[]{:S(2)}) collective-permute-start(bf16[80,128]{1,0:T(8,128)(2,1)S(1)} %shard_map.138.refs_0_), channel_id=1, source_target_pairs={{0,2},{2,4},{4,6},{6,0},{1,3},{3,5},{5,7},{7,1},{8,10},{10,12},{12... | collective-permute-start | bytes 61448 | tf_op jit(solution)/shard_map/ppermute | solution.py:38
  13.5 5.6 %collective-permute-start.5 = (bf16[80,128]{1,0:T(8,128)(2,1)S(1)}, bf16[80,128]{1,0:T(8,128)(2,1)S(1)}, u32[]{:S(2)}, u32[]{:S(2)}) collective-permute-start(bf16[80,128]{1,0:T(8,128)(2,1)S(1)} %shard_map.138.refs_0_), channel_id=1, source_target_pairs={{0,4},{2,6},{4,0},{6,2},{1,5},{3,7},{5,1},{7,3},{8,12},{10,14},{12... | collective-permute-start | bytes 61448 | tf_op jit(solution)/shard_map/ppermute | solution.py:38
  16.5 3.8 %collective-permute-start.4 = (bf16[80,128]{1,0:T(8,128)(2,1)S(1)}, bf16[80,128]{1,0:T(8,128)(2,1)S(1)}, u32[]{:S(2)}, u32[]{:S(2)}) collective-permute-start(bf16[80,128]{1,0:T(8,128)(2,1)S(1)} %shard_map.138.refs_0_), channel_id=1, source_target_pairs={{0,6},{2,0},{4,2},{6,4},{1,7},{3,1},{5,3},{7,5},{8,14},{10,8},{12,... | collective-permute-start | bytes 61448 | tf_op jit(solution)/shard_map/ppermute | solution.py:38
  20.3 14.6 %copy-start.1 = (bf16[512,4096]{1,0:T(8,128)(2,1)S(1)}, bf16[512,4096]{1,0:T(8,128)(2,1)}, u32[]{:S(2)}) copy-start(bf16[512,4096]{1,0:T(8,128)(2,1)} %w_down.1) | copy-start | bytes 12582916
  21.1 1.2 %collective-permute-start.7 = (bf16[4,512]{1,0:T(4,128)(2,1)S(1)}, bf16[4,512]{1,0:T(4,128)(2,1)S(1)}, u32[]{:S(2)}, u32[]{:S(2)}) collective-permute-start(bf16[4,512]{1,0:T(4,128)(2,1)S(1)} %get-tuple-element.14), channel_id=1, source_target_pairs={{0,1},{1,0},{2,3},{3,2},{4,5},{5,4},{6,7},{7,6},{8,9},{9,8},{10,11... | collective-permute-start | bytes 12296 | tf_op jit(solution)/shard_map/ppermute | solution.py:333
  22.2 12.7 %copy-start = (bf16[4096,512]{1,0:T(8,128)(2,1)S(1)}, bf16[4096,512]{1,0:T(8,128)(2,1)}, u32[]{:S(2)}) copy-start(bf16[4096,512]{1,0:T(8,128)(2,1)} %w_up.1) | copy-start | bytes 12582916
  22.2 12.7 %copy-start.2 = (bf16[4096]{0:T(1024)(128)(2,1)S(1)}, bf16[4096]{0:T(1024)(128)(2,1)}, u32[]{:S(2)}) copy-start(bf16[4096]{0:T(1024)(128)(2,1)} %param.24) | copy-start | bytes 24580
